TPU v7x, 32 devices: a whole 2x2x4 slice. The times are simulated.
32 devices in a mesh: grp: 2 (over y), sp: 4 (over z), tp: 4 (over x, core).
Axes of the slice: x: 2, y: 2, z: 4, core: 2. Of those that a mesh axis runs over, the one named last changes fastest.
Arguments:
- tokens_in: bfloat16 [3072, 4096], P(('grp', 'sp')), parts along dimension 0, may hold values from -6 to 6
- norm_gain: float32 [4096], replicated, may hold values from 0.1 to 1.9
- window_query: bfloat16 [4096, 1024], P('sp', 'tp'), may hold values from -0.09375 to 0.09375
- window_key: bfloat16 [4096, 512], P('sp', 'tp'), may hold values from -0.09375 to 0.09375
- window_value: bfloat16 [4096, 512], P('sp', 'tp'), may hold values from -0.09375 to 0.09375
- window_query_gain: float32 [64], replicated, may hold values from 0.6 to 16
- window_key_gain: float32 [64], replicated, may hold values from 0.6 to 16
- sink_logit: float32 [16], P('tp'), may hold values from 1 to 6
- dense_query: bfloat16 [4096, 1024], P('sp', 'tp'), may hold values from -0.09375 to 0.09375
- dense_key: bfloat16 [4096, 512], P('sp', 'tp'), may hold values from -0.09375 to 0.09375
- dense_value: bfloat16 [4096, 512], P('sp', 'tp'), may hold values from -0.09375 to 0.09375
- dense_query_gain: float32 [64], replicated, may hold values from 1 to 14
- dense_key_gain: float32 [64], replicated, may hold values from 1 to 14
- window_out: bfloat16 [1024, 4096], P('tp', 'sp'), may hold values from -1.5 to 1.5
- dense_out: bfloat16 [1024, 4096], P('tp', 'sp'), may hold values from -3 to 3
Outputs:
- mixed_out: bfloat16 [3072, 4096], P(('grp', 'sp', 'tp')), parts along dimension 0
There are 2 independent parts, one for each index of `grp`. A program takes and returns all parts, laid end to end along the dimension named above; an argument that names none is the same for every part. Nothing has to cross between parts.
All inputs are finite; a program needn't handle non-finite values.
Results may differ from a plain program's by a relative error of at most 0.03.
The roundings to bfloat16 on the way count: a program that leaves them out, or rounds other values in their place, can miss the bound.
Values may be sent and summed in bfloat16 or wider, within the bound.
A program may use at most 64 MiB of HBM per device.

v0:
```python
import jax
import jax.numpy as jnp
from jax import lax
from jax.sharding import PartitionSpec as P

HD = 64
WINDOW = 128
GRID_W = 64


EPS = 1e-06
THETA = 10000.0


def extended(block, sides, width):
    for axis, dim in sides:
        count = lax.axis_size(axis)
        forward = [(i, i + 1) for i in range(count - 1)]
        backward = [(target, source) for source, target in forward]
        low = lax.ppermute(
            lax.slice_in_dim(block, block.shape[dim] - width, None, axis=dim), axis, forward
        )
        high = lax.ppermute(lax.slice_in_dim(block, 0, width, axis=dim), axis, backward)
        block = jnp.concatenate([low, block, high], axis=dim)
    return block


def rope_table(places, width):
    inverse = THETA ** (-jnp.arange(0, width, 2, dtype=jnp.float32) / width)
    angles = places.astype(jnp.float32)[:, None] * inverse[None, :]
    angles = jnp.concatenate([angles, angles], axis=-1)
    return (jnp.cos(angles), jnp.sin(angles))


def turn(values, tables):
    cosine, sine = tables
    middle = values.shape[-1] // 2
    rotated = jnp.concatenate([-values[..., middle:], values[..., :middle]], axis=-1)
    return values * cosine[:, None, :] + rotated * sine[:, None, :]


def head_norm(projected, gain):
    width = gain.shape[0]
    heads = projected.reshape(projected.shape[0], -1, width)
    return heads * lax.rsqrt(jnp.mean(heads * heads, axis=-1, keepdims=True) + EPS) * gain


def line_heads(projected, gain, places):
    normed = head_norm(projected, gain)
    turned = turn(normed, rope_table(places, gain.shape[0]))
    return turned.reshape(projected.shape).astype(jnp.bfloat16)


def grid_heads(projected, gain, places):
    normed = head_norm(projected, gain)
    middle = gain.shape[0] // 2
    by_row = turn(normed[..., :middle], rope_table(places // GRID_W, middle))
    by_col = turn(normed[..., middle:], rope_table(places % GRID_W, middle))
    joined = jnp.concatenate([by_row, by_col], axis=-1)
    return joined.reshape(projected.shape).astype(jnp.bfloat16)


def banded(query, keys_ext, values_ext, offset, total_len, sink_logit):
    length = query.shape[0]
    kv_heads = keys_ext.shape[1] // HD
    group_size = query.shape[1] // (HD * kv_heads)
    block_count = length // WINDOW
    query_blocks = query.reshape(block_count, WINDOW, kv_heads, group_size, HD)
    key_blocks = keys_ext.reshape(block_count + 2, WINDOW, kv_heads, HD)
    value_blocks = values_ext.reshape(block_count + 2, WINDOW, kv_heads, HD)
    key_near = jnp.concatenate([key_blocks[:-2], key_blocks[1:-1], key_blocks[2:]], axis=1)
    value_near = jnp.concatenate([value_blocks[:-2], value_blocks[1:-1], value_blocks[2:]], axis=1)
    scores = jnp.einsum(
        "nqhgd,nkhd->nhgqk", query_blocks, key_near, preferred_element_type=jnp.float32
    ) * HD ** (-0.5)
    query_pos = offset + jnp.arange(length, dtype=jnp.int32).reshape(block_count, WINDOW)
    key_pos = (
        offset
        - WINDOW
        + (
            jnp.arange(block_count, dtype=jnp.int32)[:, None] * WINDOW
            + jnp.arange(3 * WINDOW, dtype=jnp.int32)[None, :]
        )
    )
    valid = (
        (jnp.abs(query_pos[:, :, None] - key_pos[:, None, :]) <= WINDOW)
        & (key_pos >= 0)[:, None, :]
        & (key_pos < total_len)[:, None, :]
    )
    scores = jnp.where(valid[:, None, None], scores, -jnp.inf)
    floor = sink_logit.reshape(kv_heads, group_size)[None, :, :, None, None]
    top = jnp.maximum(jnp.max(scores, axis=-1, keepdims=True), floor)
    expon = jnp.exp(scores - top)
    weights = (expon / (jnp.sum(expon, axis=-1, keepdims=True) + jnp.exp(floor - top))).astype(
        jnp.bfloat16
    )
    result = jnp.einsum(
        "nhgqk,nkhd->nqhgd", weights, value_near, preferred_element_type=jnp.float32
    )
    return result.astype(jnp.bfloat16).reshape(length, -1)


def dense_whole(query, keys, values):
    length = query.shape[0]
    kv_heads = keys.shape[1] // HD
    group_size = query.shape[1] // (HD * kv_heads)
    block = 128
    query_blocks = query.reshape(length // block, block, kv_heads, group_size, HD)
    key_heads = keys.reshape(-1, kv_heads, HD)
    value_heads = values.reshape(-1, kv_heads, HD)

    def one_block(query_block):
        scores = jnp.einsum(
            "qhgd,khd->hgqk", query_block, key_heads, preferred_element_type=jnp.float32
        ) * HD ** (-0.5)
        top = jnp.max(scores, axis=-1, keepdims=True)
        expon = jnp.exp(scores - top)
        total = jnp.sum(expon, axis=-1)
        summed = jnp.einsum(
            "hgqk,khd->qhgd",
            expon.astype(jnp.bfloat16),
            value_heads,
            preferred_element_type=jnp.float32,
        )
        return (summed / jnp.transpose(total, (2, 0, 1))[..., None]).astype(jnp.bfloat16)

    result = lax.map(one_block, query_blocks)
    return result.reshape(length, -1)


def local(
    tokens_in,
    norm_gain,
    window_query,
    window_key,
    window_value,
    window_query_gain,
    window_key_gain,
    sink_logit,
    dense_query,
    dense_key,
    dense_value,
    dense_query_gain,
    dense_key_gain,
    window_out,
    dense_out,
):
    length = tokens_in.shape[0]
    inputs = tokens_in.astype(jnp.float32)
    normed = (
        inputs * lax.rsqrt(jnp.mean(inputs * inputs, axis=-1, keepdims=True) + EPS) * norm_gain
    ).astype(jnp.bfloat16)
    pieces = (
        lax.all_gather(window_query, "sp", axis=0, tiled=True),
        lax.all_gather(window_key, "sp", axis=0, tiled=True),
        lax.all_gather(window_value, "sp", axis=0, tiled=True),
        lax.all_gather(dense_query, "sp", axis=0, tiled=True),
        lax.all_gather(dense_key, "sp", axis=0, tiled=True),
        lax.all_gather(dense_value, "sp", axis=0, tiled=True),
    )
    projected = tuple(
        (jnp.dot(normed, weight, preferred_element_type=jnp.float32) for weight in pieces)
    )
    offset = lax.axis_index("sp") * length
    total_len = length * lax.axis_size("sp")
    places = offset + jnp.arange(length, dtype=jnp.int32)
    query_win = line_heads(projected[0], window_query_gain, places)
    key_win = line_heads(projected[1], window_key_gain, places)
    value_win = projected[2].astype(jnp.bfloat16)
    query_den = grid_heads(projected[3], dense_query_gain, places)
    key_den = grid_heads(projected[4], dense_key_gain, places)
    value_den = projected[5].astype(jnp.bfloat16)
    framed = extended(jnp.stack([key_win, value_win]), (("sp", 1),), WINDOW)
    att_win = banded(query_win, framed[0], framed[1], offset, total_len, sink_logit)
    dense_pair = jnp.stack([key_den, value_den])
    every = lax.all_gather(dense_pair, "sp", axis=1, tiled=True)
    att_den = dense_whole(query_den, every[0], every[1])
    pieces = lax.all_gather((window_out, dense_out), "sp", axis=1, tiled=True)
    terms = jnp.dot(att_win, pieces[0], preferred_element_type=jnp.float32) + jnp.dot(
        att_den, pieces[1], preferred_element_type=jnp.float32
    )
    rounded = lax.optimization_barrier(terms.astype(jnp.bfloat16)).astype(jnp.float32)
    return lax.psum_scatter(rounded.astype(jnp.bfloat16), "tp", scatter_dimension=0, tiled=True)


def solution(mesh):
    return jax.shard_map(
        local,
        mesh=mesh,
        in_specs=(
            P(("grp", "sp"), None),
            P(),
            P("sp", "tp"),
            P("sp", "tp"),
            P("sp", "tp"),
            P(),
            P(),
            P("tp"),
            P("sp", "tp"),
            P("sp", "tp"),
            P("sp", "tp"),
            P(),
            P(),
            P("tp", "sp"),
            P("tp", "sp"),
        ),
        out_specs=P(("grp", "sp", "tp"), None),
        check_vma=False,
    )
```

profile of v0, /device:TPU:1, one launch (start us, length us, event | category | flops | bytes accessed | tf_op | source)
XLA Modules:
  0.0 366.8 jit_solution(561253262640707710)
XLA Ops:
  18.1 3.0 fusion.28
  21.1 1.7 fusion.36
  22.8 15.7 %all-gather.19.cloned.1.call-done = bf16[4096,128]{1,0:T(8,128)(2,1)} async-done(((bf16[1024,128]{1,0:T(8,128)(2,1)}), bf16[4096,128]{1,0:T(8,128)(2,1)}) %all-gather.19.cloned.1.call-update) | async-done | bytes 1048592 | tf_op jit(solution)/shard_map/all_gather | solution.py:158
  38.5 2.2 multiply_reduce_fusion.2
  41.1 26.3 %all-gather.21.cloned.1.call-done = bf16[4096,128]{1,0:T(8,128)(2,1)} async-done(((bf16[1024,128]{1,0:T(8,128)(2,1)}), bf16[4096,128]{1,0:T(8,128)(2,1)}) %all-gather.21.cloned.1.call-update) | async-done | bytes 1048592 | tf_op jit(solution)/shard_map/all_gather | solution.py:159
  67.5 2.2 fusion.34
  69.7 21.3 %all_gather.34 = bf16[2,1536,128]{2,1,0:T(8,128)(2,1)} all-gather(bf16[2,384,128]{2,1,0:T(8,128)(2,1)S(1)} %pad_maximum_fusion.1), channel_id=1, replica_groups=mesh['grp'=2,'sp'=4,'tp'=4] {'sp'}, dimensions={1}, use_global_device_ids=true | all-gather | bytes 983040 | tf_op jit(solution)/shard_map/all_gather | solution.py:176
  91.0 12.6 %all-gather.9.cloned.1.call-done = bf16[4096,128]{1,0:T(8,128)(2,1)} async-done(((bf16[1024,128]{1,0:T(8,128)(2,1)}), bf16[4096,128]{1,0:T(8,128)(2,1)}) %all-gather.9.cloned.1.call-update) | async-done | bytes 1048592 | tf_op jit(solution)/shard_map/all_gather | solution.py:155
  103.6 2.2 multiply_reduce_fusion.3
  106.1 26.3 %all-gather.11.cloned.1.call-done = bf16[4096,128]{1,0:T(8,128)(2,1)} async-done(((bf16[1024,128]{1,0:T(8,128)(2,1)}), bf16[4096,128]{1,0:T(8,128)(2,1)}) %all-gather.11.cloned.1.call-update) | async-done | bytes 1048592 | tf_op jit(solution)/shard_map/all_gather | solution.py:156
  132.4 2.3 convolution_convert_fusion.1
  135.4 3.4 collective-permute-start
  143.8 1.9 copy.40
  148.8 1.7 pad_maximum_fusion.7
  150.6 1.6 slice.124
  153.7 1.6 slice.127
  156.9 1.6 slice.118
  160.0 1.6 slice.122
  163.2 16.9 %all-gather.17.cloned.1.call-done = bf16[4096,256]{1,0:T(8,128)(2,1)} async-done(((bf16[1024,256]{1,0:T(8,128)(2,1)}), bf16[4096,256]{1,0:T(8,128)(2,1)}) %all-gather.17.cloned.1.call-update) | async-done | bytes 2097168 | tf_op jit(solution)/shard_map/all_gather | solution.py:157
  180.0 2.9 multiply_reduce_fusion
  183.9 1.7 convert_element_type.89
  185.6 1.7 copy.41
  187.3 10.5 %while.10 = (s32[]{:T(128)}, bf16[3,128,2,2,64]{1,4,3,2,0:T(8,128)(2,1)}, bf16[3,128,2,2,64]{1,4,3,2,0:T(8,128)(2,1)}, bf16[1536,2,64]{0,2,1:T(8,128)(2,1)S(1)}, bf16[1536,2,64]{0,2,1:T(8,128)(2,1)}, /*index=5*/s32[]{:T(128)}) while((s32[]{:T(128)}, bf16[3,128,2,2,64]{1,4,3,2,0:T(8,128)(2,1)}, bf16[3,128,2,2,64]{1,4,3,2,0:T(8,128)(2,1)}, ...), condition=%wide.region_10.11_spmd, body=%wide.region_7.10_spmd.sunk | while | flops 206109696 | bytes 11938913 | solution.py:127
  187.3 1.6 fusion.105
  194.3 1.6 fusion.105
  198.9 26.2 %all-gather.13.cloned.1.call-done = bf16[4096,256]{1,0:T(8,128)(2,1)} async-done(((bf16[1024,256]{1,0:T(8,128)(2,1)}), bf16[4096,256]{1,0:T(8,128)(2,1)}) %all-gather.13.cloned.1.call-update) | async-done | bytes 2097168 | tf_op jit(solution)/shard_map/all_gather | solution.py:154
  225.1 2.9 multiply_reduce_fusion.1
  231.3 39.9 %all-gather.15.cloned.1.call-done = bf16[256,4096]{1,0:T(8,128)(2,1)} async-done(((bf16[256,1024]{1,0:T(8,128)(2,1)}), bf16[256,4096]{1,0:T(8,128)(2,1)}) %all-gather.15.cloned.1.call-update) | async-done | bytes 2097168 | tf_op jit(solution)/shard_map/all_gather | solution.py:178
  271.2 5.3 %fusion.50 = f32[384,4096]{1,0:T(8,128)} fusion(bf16[256,4096]{1,0:T(8,128)(2,1)} %all-gather.15.cloned.1.call-done, bf16[32,8,3,128]{3,2,1,0:T(4,128)(2,1)S(1)} %bitcast.171), kind=kOutput, calls=%fused_computation.60 | convolution fusion | flops 805306368 | bytes 8585216 | tf_op jit(solution)/shard_map/dot_general | solution.py:179
  276.5 40.8 %all-gather.23.cloned.1.call-done = bf16[256,4096]{1,0:T(8,128)(2,1)} async-done(((bf16[256,1024]{1,0:T(8,128)(2,1)}), bf16[256,4096]{1,0:T(8,128)(2,1)}) %all-gather.23.cloned.1.call-update) | async-done | bytes 2097168 | tf_op jit(solution)/shard_map/all_gather | solution.py:178
  317.2 6.1 %add_convert_fusion = bf16[384,4096]{1,0:T(8,128)(2,1)} fusion(f32[384,4096]{1,0:T(8,128)} %fusion.50, bf16[256,4096]{1,0:T(8,128)(2,1)} %all-gather.23.cloned.1.call-done, bf16[32,8,3,128]{3,2,1,0:T(4,128)(2,1)S(1)} %bitcast.170), kind=kOutput, calls=%fused_computation.22 | convolution fusion | flops 808452096 | bytes 11730944 | tf_op jit(solution)/shard_map/dot_general | solution.py:179
  323.4 36.8 %reduce-scatter.2.cloned.1.call-done = bf16[96,4096]{1,0:T(8,128)(2,1)} async-done(((bf16[384,4096]{1,0:T(8,128)(2,1)}), bf16[96,4096]{1,0:T(8,128)(2,1)}) %reduce-scatter.2.cloned.1.call-update) | async-done | bytes 786448 | tf_op jit(solution)/shard_map/reduce_scatter | solution.py:183
  (160 shorter events, 39.4 us)
Async XLA Ops:
  6.5 6.3 %copy-start.1 = (bf16[384,4096]{1,0:T(8,128)(2,1)S(1)}, bf16[384,4096]{1,0:T(8,128)(2,1)}, u32[]{:S(2)}) copy-start(bf16[384,4096]{1,0:T(8,128)(2,1)} %param.17) | copy-start | bytes 9437188
  6.5 32.0 %all-gather.19.cloned.1.call-start = ((), (), s32[]{:S(2)}) async-start(), calls=%async_computation.6 | async-start | bytes 1310720 | tf_op jit(solution)/shard_map/all_gather | solution.py:158
  7.3 60.2 %all-gather.21.cloned.1.call-start = ((), (), s32[]{:S(2)}) async-start(), calls=%async_computation.7 | async-start | bytes 1310720 | tf_op jit(solution)/shard_map/all_gather | solution.py:159
  8.0 95.5 %all-gather.9.cloned.1.call-start = ((), (), s32[]{:S(2)}) async-start(), calls=%async_computation.1 | async-start | bytes 1310720 | tf_op jit(solution)/shard_map/all_gather | solution.py:155
  8.7 123.7 %all-gather.11.cloned.1.call-start = ((), (), s32[]{:S(2)}) async-start(), calls=%async_computation.2 | async-start | bytes 1310720 | tf_op jit(solution)/shard_map/all_gather | solution.py:156
  9.3 170.7 %all-gather.17.cloned.1.call-start = ((), (), s32[]{:S(2)}) async-start(), calls=%async_computation.5 | async-start | bytes 2621440 | tf_op jit(solution)/shard_map/all_gather | solution.py:157
  9.9 215.2 %all-gather.13.cloned.1.call-start = ((), (), s32[]{:S(2)}) async-start(), calls=%async_computation.3 | async-start | bytes 2621440 | tf_op jit(solution)/shard_map/all_gather | solution.py:154
  10.5 260.7 %all-gather.15.cloned.1.call-start = ((), (), s32[]{:S(2)}) async-start(), calls=%async_computation.4 | async-start | bytes 2621440 | tf_op jit(solution)/shard_map/all_gather | solution.py:178
  11.2 306.0 %all-gather.23.cloned.1.call-start = ((), (), s32[]{:S(2)}) async-start(), calls=%async_computation.8 | async-start | bytes 2621440 | tf_op jit(solution)/shard_map/all_gather | solution.py:178
  12.0 348.3 %reduce-scatter.2.cloned.1.call-start = ((), (), s32[]{:S(2)}) async-start(), calls=%async_computation.9 | async-start | bytes 3932160 | tf_op jit(solution)/shard_map/reduce_scatter | solution.py:183
  13.7 27.2 %copy-start.10 = (f32[384,32]{0,1:T(8,128)}, f32[384,32]{0,1:T(8,128)S(1)}, u32[]{:S(2)}) copy-start(f32[384,32]{0,1:T(8,128)S(1)} %get-tuple-element.83) | copy-start | bytes 147460
  13.7 27.2 %copy-start.12 = (f32[384,32]{0,1:T(8,128)}, f32[384,32]{0,1:T(8,128)S(1)}, u32[]{:S(2)}) copy-start(f32[384,32]{0,1:T(8,128)S(1)} %get-tuple-element.84) | copy-start | bytes 147460
  13.9 27.0 %copy-start.14 = (f32[384,32]{0,1:T(8,128)}, f32[384,32]{0,1:T(8,128)S(1)}, u32[]{:S(2)}) copy-start(f32[384,32]{0,1:T(8,128)S(1)} %get-tuple-element.85) | copy-start | bytes 147460
  13.9 27.0 %copy-start.16 = (f32[384,32]{0,1:T(8,128)}, f32[384,32]{0,1:T(8,128)S(1)}, u32[]{:S(2)}) copy-start(f32[384,32]{0,1:T(8,128)S(1)} %get-tuple-element.86) | copy-start | bytes 147460
  14.1 91.8 %copy-start.7 = (f32[384,64]{0,1:T(8,128)}, f32[384,64]{0,1:T(8,128)S(1)}, u32[]{:S(2)}) copy-start(f32[384,64]{0,1:T(8,128)S(1)} %get-tuple-element.82) | copy-start | bytes 294916
  14.2 91.8 %copy-start.5 = (f32[384,64]{0,1:T(8,128)}, f32[384,64]{0,1:T(8,128)S(1)}, u32[]{:S(2)}) copy-start(f32[384,64]{0,1:T(8,128)S(1)} %get-tuple-element.81) | copy-start | bytes 294916
  21.1 19.7 %copy-start.29 = (f32[64]{0:T(128)S(1)}, f32[64]{0:T(128)}, u32[]{:S(2)}) copy-start(f32[64]{0:T(128)} %param.29) | copy-start | bytes 772
  69.7 36.1 %copy-start.30 = (f32[64]{0:T(128)S(1)}, f32[64]{0:T(128)}, u32[]{:S(2)}) copy-start(f32[64]{0:T(128)} %param.23) | copy-start | bytes 772
  69.7 36.3 %copy-start.32 = (f32[128]{0:T(128)S(1)}, f32[128]{0:T(128)}, u32[]{:S(2)}) copy-start(f32[128]{0:T(128)} %mul.364) | copy-start | bytes 1540
  106.1 35.8 %copy-start.3 = (bf16[384,128]{0,1:T(8,128)(2,1)}, bf16[384,128]{0,1:T(8,128)(2,1)S(1)}, u32[]{:S(2)}) copy-start(bf16[384,128]{0,1:T(8,128)(2,1)S(1)} %fusion.57) | copy-start | bytes 294916
  132.4 7.8 %copy-start.2 = (bf16[2,1536,128]{2,1,0:T(8,128)(2,1)S(1)}, bf16[2,1536,128]{2,1,0:T(8,128)(2,1)}, u32[]{:S(2)}) copy-start(bf16[2,1536,128]{2,1,0:T(8,128)(2,1)} %all_gather.34) | copy-start | bytes 2359300
  134.7 7.9 %copy-start.4 = (bf16[384,128]{0,1:T(8,128)(2,1)}, bf16[384,128]{0,1:T(8,128)(2,1)S(1)}, u32[]{:S(2)}) copy-start(bf16[384,128]{0,1:T(8,128)(2,1)S(1)} %convolution_convert_fusion.1) | copy-start | bytes 294916
  135.4 13.4 %collective-permute-start = (bf16[2,128,128]{1,2,0:T(8,128)(2,1)}, bf16[2,128,128]{1,2,0:T(8,128)(2,1)}, u32[]{:S(2)}, u32[]{:S(2)}) collective-permute-start(bf16[2,128,128]{1,2,0:T(8,128)(2,1)} %get-tuple-element.77), channel_id=1, source_target_pairs={{0,4},{4,8},{8,12},{1,5},{5,9},{9,13},{2,6},{6,10},{10,14},{3,7},{... | collective-permute-start | bytes 196616 | tf_op jit(solution)/shard_map/ppermute | solution.py:20
  138.8 10.1 %collective-permute-start.1 = (bf16[2,128,128]{1,2,0:T(8,128)(2,1)}, bf16[2,128,128]{1,2,0:T(8,128)(2,1)}, u32[]{:S(2)}, u32[]{:S(2)}) collective-permute-start(bf16[2,128,128]{1,2,0:T(8,128)(2,1)} %get-tuple-element.78), channel_id=1, source_target_pairs={{4,0},{8,4},{12,8},{5,1},{9,5},{13,9},{6,2},{10,6},{14,10},{7,3},{... | collective-permute-start | bytes 196616 | tf_op jit(solution)/shard_map/ppermute | solution.py:23
  163.2 19.8 %copy-start.31 = (f32[64]{0:T(128)S(1)}, f32[64]{0:T(128)}, u32[]{:S(2)}) copy-start(f32[64]{0:T(128)} %param.28) | copy-start | bytes 772
  180.0 3.1 copy-start.13
  180.0 3.1 copy-start.15
  180.0 3.1 copy-start.17
  198.9 29.2 %copy-start.28 = (f32[64]{0:T(128)S(1)}, f32[64]{0:T(128)}, u32[]{:S(2)}) copy-start(f32[64]{0:T(128)} %param.22) | copy-start | bytes 772
  198.9 29.4 %copy-start.6 = (f32[384,64]{0,1:T(8,128)S(1)}, f32[384,64]{0,1:T(8,128)}, u32[]{:S(2)}) copy-start(f32[384,64]{0,1:T(8,128)} %copy-done.5) | copy-start | bytes 294916
  198.9 29.4 %copy-start.26 = (f32[256]{0:T(256)S(1)}, f32[256]{0:T(256)}, u32[]{:S(2)}) copy-start(f32[256]{0:T(256)} %mul.387) | copy-start | bytes 3076
  225.1 3.2 copy-start.8
  (14 other events, 24.7 us)
Sparse Core Ops, SparseCore 0:
  8.9 29.5 all-gather.18
  40.1 27.3 all-gather.20
  69.0 34.4 all-gather.8
  105.0 27.3 all-gather.10
  133.8 46.1 all-gather.16
  181.5 43.6 all-gather.12
  226.7 44.4 all-gather.14
  272.8 44.4 all-gather.22
  323.5 36.6 reduce-scatter.1
where the time goes:
time: 369 us; the launch traced here: 367 us
  waiting for transfers between devices  247 us (67%)
  matrix products  36.2 us (10%)
  local copies, waits for them, and re-layouts  30.6 us (8%)
  blocking collectives  21.3 us (6%)
  between operations  13.9 us (4%)
  other arithmetic  13.2 us (4%)
  starting transfers between devices  5.14 us (1%)
    all_gather x2, waiting for transfers between devices, local(): pieces = lax.all_gather((window_out, dense_out), 'sp', axis=1, tiled=True)  80.6 us
    reduce_scatter x1, waiting for transfers between devices, local(): lax.psum_scatter(rounded.astype(jnp.bfloat16), 'tp', scatter_dimension=0,...  36.8 us
    all_gather x1, waiting for transfers between devices, local(): lax.all_gather(dense_value, 'sp', axis=0, tiled=True)  26.3 us
    all_gather x1, waiting for transfers between devices, local(): lax.all_gather(window_value, 'sp', axis=0, tiled=True)  26.3 us
    all_gather x1, waiting for transfers between devices, local(): lax.all_gather(window_query, 'sp', axis=0, tiled=True)  26.2 us
    all_gather x1, blocking collectives, local(): every = lax.all_gather(dense_pair, 'sp', axis=1, tiled=True)  21.3 us
    all_gather x1, waiting for transfers between devices, local(): lax.all_gather(dense_query, 'sp', axis=0, tiled=True)  16.9 us
    all_gather x1, waiting for transfers between devices, local(): lax.all_gather(dense_key, 'sp', axis=0, tiled=True)  15.7 us
  transfers between devices with their start and end apart: 11, of which 9 were waited for; matrix products, arithmetic and copies ran while one was open for 20% of the time, Pallas kernels for 0%

commit v1 on v0

--- a/solution.py
+++ b/solution.py
@@ -1,6 +1,8 @@
 import jax
 import jax.numpy as jnp
 from jax import lax
+from jax.experimental import pallas as pl
+from jax.experimental.pallas import tpu as pltpu
 from jax.sharding import PartitionSpec as P
 
 HD = 64
@@ -126,6 +128,193 @@
 
     result = lax.map(one_block, query_blocks)
     return result.reshape(length, -1)
+
+
+MESH = pl.DeviceIdType.MESH
+HALVES = 2
+
+
+class LineGather:
+    def __init__(self, own, buf, z_recv, y_recv, r_send, l_send, y_send):
+        self.own, self.buf = own, buf
+        self.z_recv, self.y_recv = z_recv, y_recv
+        self.r_send, self.l_send, self.y_send = r_send, l_send, y_send
+        self.n = lax.axis_size("sp")
+        self.s = lax.axis_index("sp")
+        self.g = lax.axis_index("grp")
+        self.chunks = z_recv.shape[1]
+        self.half = own.shape[0] // HALVES
+        self.size = self.half // self.chunks
+
+    def rows(self, half, c):
+        return pl.ds(pl.multiple_of(half * self.half + c * self.size, self.size), self.size)
+
+    def copy(self, src, o, c, sem, recv, target, half):
+        return pltpu.make_async_remote_copy(
+            src_ref=src,
+            dst_ref=self.buf.at[o, self.rows(half, c)],
+            send_sem=sem.at[o, c],
+            recv_sem=recv.at[o, c],
+            device_id=target,
+            device_id_type=MESH,
+        )
+
+    def right(self, src, o, c):
+        return self.copy(src, o, c, self.r_send, self.z_recv, {"sp": lax.rem(self.s + 1, self.n)}, self.g)
+
+    def left(self, src, o, c):
+        return self.copy(
+            src, o, c, self.l_send, self.z_recv, {"sp": lax.rem(self.s + self.n - 1, self.n)}, self.g
+        )
+
+    def twin(self, o, c, half):
+        return self.copy(
+            self.buf.at[o, self.rows(half, c)], o, c, self.y_send, self.y_recv, {"grp": 1 - self.g}, half
+        )
+
+    def start(self):
+        for c in range(self.chunks):
+            mine = self.own.at[self.rows(self.g, c)]
+
+            @pl.when(self.s + 1 < self.n)
+            def _():
+                self.right(mine, self.s, c).start()
+
+            @pl.when(self.s > 0)
+            def _():
+                self.left(mine, self.s, c).start()
+
+    def forward(self, d):
+        for c in range(self.chunks):
+
+            @pl.when(self.s - d >= 0)
+            def _():
+                o = self.s - d
+                there = self.buf.at[o, self.rows(self.g, c)]
+                self.right(there, o, c).wait_recv()
+
+                @pl.when(self.s + 1 < self.n)
+                def _():
+                    self.right(there, o, c).start()
+
+                self.twin(o, c, self.g).start()
+
+            @pl.when(self.s + d < self.n)
+            def _():
+                o = self.s + d
+                there = self.buf.at[o, self.rows(self.g, c)]
+                self.left(there, o, c).wait_recv()
+
+                @pl.when(self.s > 0)
+                def _():
+                    self.left(there, o, c).start()
+
+                self.twin(o, c, self.g).start()
+
+    def use(self, d, fn):
+        @pl.when(self.s - d >= 0)
+        def _():
+            for c in range(self.chunks):
+                self.twin(self.s - d, c, 1 - self.g).wait_recv()
+            fn(self.s - d)
+
+        @pl.when(self.s + d < self.n)
+        def _():
+            for c in range(self.chunks):
+                self.twin(self.s + d, c, 1 - self.g).wait_recv()
+            fn(self.s + d)
+
+    def run(self, fn):
+        self.forward(1)
+
+        @pl.loop(2, self.n)
+        def _(d):
+            self.forward(d)
+            self.use(d - 1, fn)
+
+        self.use(self.n - 1, fn)
+
+    def finish(self):
+        @pl.loop(0, self.n)
+        def _(o):
+            for c in range(self.chunks):
+                there = self.buf.at[o, self.rows(self.g, c)]
+
+                @pl.when((o <= self.s) & (self.s + 1 < self.n))
+                def _():
+                    self.right(there, o, c).wait_send()
+
+                @pl.when((o >= self.s) & (self.s > 0))
+                def _():
+                    self.left(there, o, c).wait_send()
+
+                @pl.when(o != self.s)
+                def _():
+                    self.twin(o, c, self.g).wait_send()
+
+
+def greet_line():
+    n, s, g = lax.axis_size("sp"), lax.axis_index("sp"), lax.axis_index("grp")
+    barrier = pltpu.get_barrier_semaphore()
+    pl.semaphore_signal(barrier, inc=1, device_id={"grp": 1 - g}, device_id_type=MESH)
+
+    @pl.when(s + 1 < n)
+    def _():
+        pl.semaphore_signal(barrier, inc=1, device_id={"sp": lax.rem(s + 1, n)}, device_id_type=MESH)
+
+    @pl.when(s > 0)
+    def _():
+        pl.semaphore_signal(barrier, inc=1, device_id={"sp": lax.rem(s + n - 1, n)}, device_id_type=MESH)
+
+    pl.semaphore_wait(barrier, 1 + (s + 1 < n).astype(jnp.int32) + (s > 0).astype(jnp.int32))
+
+
+def project_kernel(x_ref, w_ref, wo_ref, proj_ref, wo_all, wbuf, *sems):
+    s = lax.axis_index("sp")
+    depth = w_ref.shape[0]
+    into = LineGather(w_ref, wbuf, *sems[:5])
+    out = LineGather(wo_ref, wo_all, *sems[5:])
+    greet_line()
+    into.start()
+
+    def columns(o):
+        return pl.ds(pl.multiple_of(o * depth, depth), depth)
+
+    proj_ref[...] = jnp.dot(x_ref[:, columns(s)], w_ref[...], preferred_element_type=jnp.float32)
+
+    def add(o):
+        proj_ref[...] += jnp.dot(x_ref[:, columns(o)], wbuf[o], preferred_element_type=jnp.float32)
+
+    into.run(add)
+    out.start()
+    wo_all[s] = wo_ref[...]
+    out.run(lambda o: None)
+    into.finish()
+    out.finish()
+
+
+def gather_sems(n, chunks):
+    return [pltpu.SemaphoreType.DMA((n, chunks)) for _ in range(5)]
+
+
+def project(normed, weight, weight_out):
+    n = lax.axis_size("sp")
+    chunks = 4 if n <= 4 else 1
+    return pl.pallas_call(
+        project_kernel,
+        out_shape=(
+            jax.ShapeDtypeStruct((normed.shape[0], weight.shape[1]), jnp.float32),
+            jax.ShapeDtypeStruct((n,) + weight_out.shape, jnp.bfloat16),
+        ),
+        in_specs=[pl.BlockSpec(memory_space=pltpu.VMEM)] * 3,
+        out_specs=[pl.BlockSpec(memory_space=pltpu.VMEM)] * 2,
+        scratch_shapes=[pltpu.VMEM((n,) + weight.shape, jnp.bfloat16)]
+        + gather_sems(n, chunks)
+        + gather_sems(n, chunks),
+        compiler_params=pltpu.CompilerParams(
+            collective_id=0, has_side_effects=True, vmem_limit_bytes=60 * 1024 * 1024
+        ),
+    )(normed, weight, weight_out)
 
 
 def local(
@@ -150,17 +339,13 @@
     normed = (
         inputs * lax.rsqrt(jnp.mean(inputs * inputs, axis=-1, keepdims=True) + EPS) * norm_gain
     ).astype(jnp.bfloat16)
-    pieces = (
-        lax.all_gather(window_query, "sp", axis=0, tiled=True),
-        lax.all_gather(window_key, "sp", axis=0, tiled=True),
-        lax.all_gather(window_value, "sp", axis=0, tiled=True),
-        lax.all_gather(dense_query, "sp", axis=0, tiled=True),
-        lax.all_gather(dense_key, "sp", axis=0, tiled=True),
-        lax.all_gather(dense_value, "sp", axis=0, tiled=True),
-    )
-    projected = tuple(
-        (jnp.dot(normed, weight, preferred_element_type=jnp.float32) for weight in pieces)
-    )
+    weights = (window_query, window_key, window_value, dense_query, dense_key, dense_value)
+    weight_out = jnp.concatenate([window_out, dense_out], axis=0)
+    joined, out_all = project(normed, jnp.concatenate(weights, axis=1), weight_out)
+    projected, at = [], 0
+    for weight in weights:
+        projected.append(joined[:, at : at + weight.shape[1]])
+        at += weight.shape[1]
     offset = lax.axis_index("sp") * length
     total_len = length * lax.axis_size("sp")
     places = offset + jnp.arange(length, dtype=jnp.int32)
@@ -175,10 +360,9 @@
     dense_pair = jnp.stack([key_den, value_den])
     every = lax.all_gather(dense_pair, "sp", axis=1, tiled=True)
     att_den = dense_whole(query_den, every[0], every[1])
-    pieces = lax.all_gather((window_out, dense_out), "sp", axis=1, tiled=True)
-    terms = jnp.dot(att_win, pieces[0], preferred_element_type=jnp.float32) + jnp.dot(
-        att_den, pieces[1], preferred_element_type=jnp.float32
-    )
+    att = jnp.concatenate([att_win, att_den], axis=1)
+    terms = jnp.einsum("tk,nkc->tnc", att, out_all, preferred_element_type=jnp.float32)
+    terms = terms.reshape(length, -1)
     rounded = lax.optimization_barrier(terms.astype(jnp.bfloat16)).astype(jnp.float32)
     return lax.psum_scatter(rounded.astype(jnp.bfloat16), "tp", scatter_dimension=0, tiled=True)
 

time: 369 us -> 255 us (0.69)
  waiting for transfers between devices: 247 us -> 43.8 us
  Pallas kernels: 0 us -> 120 us
  matrix products: 36.2 us -> 12 us
  local copies, waits for them, and re-layouts: 30.6 us -> 23.8 us
  other arithmetic: 13.2 us -> 19 us
  blocking collectives: 21.3 us -> 16.8 us
    all_gather x8 -> x0, waiting for transfers between devices: 205 us -> none  [the longest x2 80.6 us: local(): pieces = lax.all_gather((window_out, dense_out), 'sp', axis=1, tiled=True)]
    pallas_call x0 -> x1, Pallas kernels: none -> 120 us  [project(): pl.pallas_call(project_kernel, out_shape=(jax.ShapeDtypeStruct((normed.sh...]
    dot_general x8 -> x1, matrix products: 26.2 us -> 5.65 us  [local(): jnp.einsum('tk,nkc->tnc', att, out_all, preferred_element_type=jnp.float32)]
    reduce_scatter x1, waiting for transfers between devices: 36.8 us -> 43.8 us  [local(): lax.psum_scatter(rounded.astype(jnp.bfloat16), 'tp', scatter_dimension=0,...]
    unnamed x64 -> x74, local copies, waits for them, and re-layouts: 0.71 us -> 6.35 us
    unnamed x9 -> x1, waiting for transfers between devices: 5.07 us -> 0.02 us
    all_gather x1, blocking collectives: 21.3 us -> 16.8 us  [local(): every = lax.all_gather(dense_pair, 'sp', axis=1, tiled=True)]
  transfers between devices with their start and end apart: 11 -> 3, of which waited for: 9 -> 1; matrix products, arithmetic and copies ran while one was open for 20% -> 9% of each run, Pallas kernels for 0% -> 0%
where the time goes in v1:
time: 255 us; the launch traced here: 253 us
  Pallas kernels  120 us (47%)
  waiting for transfers between devices  43.8 us (17%)
  local copies, waits for them, and re-layouts  23.8 us (9%)
  other arithmetic  19 us (7%)
  blocking collectives  16.8 us (7%)
  between operations  14.3 us (6%)
  matrix products  12 us (5%)
  starting transfers between devices  3.91 us (2%)
    pallas_call x1, Pallas kernels, project(): pl.pallas_call(project_kernel, out_shape=(jax.ShapeDtypeStruct((normed.sh...  120 us
    reduce_scatter x1, waiting for transfers between devices, local(): lax.psum_scatter(rounded.astype(jnp.bfloat16), 'tp', scatter_dimension=0,...  43.8 us
    all_gather x1, blocking collectives, local(): every = lax.all_gather(dense_pair, 'sp', axis=1, tiled=True)  16.8 us
    unnamed x74, local copies, waits for them, and re-layouts  6.35 us
    dot_general x1, matrix products, local(): jnp.einsum('tk,nkc->tnc', att, out_all, preferred_element_type=jnp.float32)  5.65 us
  transfers between devices with their start and end apart: 3, of which 1 were waited for; matrix products, arithmetic and copies ran while one was open for 9% of the time, Pallas kernels for 0%

profile of v1, /device:TPU:1, one launch (start us, length us, event | category | flops | bytes accessed | tf_op | source)
XLA Modules:
  0.0 253.3 jit_solution(14833807015797260446)
XLA Ops:
  6.6 1.2 constant_dynamic-update-slice_fusion.5
  7.8 2.7 %fusion.26 = f32[384]{0:T(512)S(1)} fusion(bf16[384,4096]{1,0:T(8,128)(2,1)} %param.17), kind=kLoop, calls=%fused_computation.19 | loop fusion | flops 4718208 | bytes 3147264 | tf_op jit(solution)/shard_map/reduce_sum | solution.py:340
  11.0 1.4 copy-done
  12.3 2.7 %fusion.28.x_ref = bf16[384,4096]{1,0:T(8,128)(2,1)} fusion(bf16[384,4096]{1,0:T(8,128)(2,1)S(1)} %copy-done, f32[4096]{0:T(1024)S(1)} %copy-done.27, f32[384]{0:T(512)S(1)} %add_rsqrt_fusion.4), kind=kLoop, calls=%fused_computation.21 | loop fusion | flops 6291456 | bytes 6309376 | tf_op jit(solution)/shard_map/convert_element_type | solution.py:341
  15.1 1.0 pad_maximum_fusion.wo_ref
  16.1 119.6 %shard_map.145 = (f32[384,1024]{1,0:T(8,128)}, bf16[4,512,1024]{2,1,0:T(8,128)(2,1)}) custom-call(bf16[384,4096]{1,0:T(8,128)(2,1)} %fusion.28.x_ref, bf16[1024,1024]{1,0:T(8,128)(2,1)} %copy-done.2, bf16[512,1024]{1,0:T(8,128)(2,1)} %pad_maximum_fusion.wo_ref), custom_call_target="tpu_custom_call" | custom-call | tf_op jit(solution)/shard_map/pallas_call | solution.py:303
  135.7 0.9 slice.134
  136.6 1.5 convert.16
  139.3 0.7 fusion.76
  140.8 2.6 %collective-permute-start = (bf16[2,128,128]{2,1,0:T(8,128)(2,1)}, bf16[2,128,128]{2,1,0:T(8,128)(2,1)}, u32[]{:S(2)}, u32[]{:S(2)}) collective-permute-start(bf16[2,128,128]{2,1,0:T(8,128)(2,1)} %get-tuple-element.87), channel_id=1, source_target_pairs={{0,4},{4,8},{8,12},{1,5},{5,9},{9,13},{2,6},{6,10},{10,14},{3,7},{... | collective-permute-start | bytes 196616 | tf_op jit(solution)/shard_map/ppermute | solution.py:22
  143.5 1.3 collective-permute-start.1
  149.2 0.7 multiply_multiply_fusion.2
  150.0 0.8 broadcast_multiply_fusion.2
  151.6 16.8 %all_gather.3 = bf16[2,1536,128]{2,1,0:T(8,128)(2,1)S(1)} all-gather(bf16[2,384,128]{2,1,0:T(8,128)(2,1)S(1)} %pad_maximum_fusion.2), channel_id=1, replica_groups=mesh['grp'=2,'sp'=4,'tp'=4] {'sp'}, dimensions={1}, use_global_device_ids=true | all-gather | bytes 983040 | tf_op jit(solution)/shard_map/all_gather | solution.py:361
  168.4 0.9 fusion.77
  169.4 1.2 copy.89
  170.5 1.2 copy.90
  171.7 1.0 add_convert_fusion
  172.7 1.2 copy.86
  173.9 0.8 multiply_multiply_fusion
  175.1 6.0 %while.10 = (s32[]{:T(128)}, bf16[3,128,2,2,64]{1,4,3,2,0:T(8,128)(2,1)S(1)}, bf16[3,128,2,2,64]{1,4,3,2,0:T(8,128)(2,1)S(1)}, bf16[1536,2,64]{0,2,1:T(8,128)(2,...) while((s32[]{:T(128)}, bf16[3,128,2,2,64]{1,4,3,2,0:T(8,128)(2,1)S(1)}, ...), condition=%wide.region_10.11_spmd, body=%wide.region_7.10_spmd.sunk | while | flops 206109696 | bytes 10365005 | solution.py:129
  176.4 0.7 fusion.88
  181.1 0.7 fusion.35
  182.6 0.8 copy.70
  184.2 0.8 pad_maximum_fusion.8
  185.5 0.8 copy.77
  186.3 1.4 fusion.30
  189.0 0.7 fusion.33
  190.6 5.7 %convolution_convert_fusion = bf16[384,4,1024]{2,0,1:T(8,128)(2,1)} fusion(bf16[4,512,1024]{2,1,0:T(8,128)(2,1)} %get-tuple-element.36, bf16[384,256]{1,0:T(8,128)(2,1)S(1)} %reshape.425, bf16[384,256]{1,0:T(8,128)(2,1)S(1)} %reshape.424), kind=kOutput, calls=%fused_computation.25 | convolution fusion | flops 1612972032 | bytes 7733248 | tf_op jit(solution)/shard_map/tk,nkc->tnc/dot_general | solution.py:364
  196.3 3.4 %copy.95 = bf16[384,4,1024]{0,2,1:T(8,128)(2,1)S(1)} copy(bf16[384,4,1024]{2,0,1:T(8,128)(2,1)} %convolution_convert_fusion) | data formatting | bytes 6291456 | tf_op jit(solution)/shard_map/convert_element_type | solution.py:366
  199.7 2.9 %copy.118 = bf16[384,4096]{1,0:T(8,128)(2,1)} copy(bf16[384,4096]{0,1:T(8,128)(2,1)S(1)} %bitcast.109) | data formatting | bytes 6291456
  202.6 43.8 %reduce-scatter.4.cloned.1.call-done = bf16[96,4096]{1,0:T(8,128)(2,1)} async-done(((bf16[384,4096]{1,0:T(8,128)(2,1)}), bf16[96,4096]{1,0:T(8,128)(2,1)}) %reduce-scatter.4.cloned.1.call-update) | async-done | bytes 786448 | tf_op jit(solution)/shard_map/reduce_scatter | solution.py:367
  (161 shorter events, 17.0 us)
Async XLA Ops:
  6.5 3.9 %copy-start.21 = (bf16[1024,128]{1,0:T(8,128)(2,1)S(1)}, bf16[1024,128]{1,0:T(8,128)(2,1)}, u32[]{:S(2)}) copy-start(bf16[1024,128]{1,0:T(8,128)(2,1)} %param.20) | copy-start | bytes 786436
  6.5 239.9 %reduce-scatter.4.cloned.1.call-start = ((), (), s32[]{:S(2)}) async-start(), calls=%async_computation.1 | async-start | bytes 3932160 | tf_op jit(solution)/shard_map/reduce_scatter | solution.py:367
  6.6 4.0 %copy-start.22 = (bf16[1024,128]{1,0:T(8,128)(2,1)S(1)}, bf16[1024,128]{1,0:T(8,128)(2,1)}, u32[]{:S(2)}) copy-start(bf16[1024,128]{1,0:T(8,128)(2,1)} %param.21) | copy-start | bytes 786436
  7.7 2.9 %copy-start.8 = (bf16[1024,256]{1,0:T(8,128)(2,1)S(1)}, bf16[1024,256]{1,0:T(8,128)(2,1)}, u32[]{:S(2)}) copy-start(bf16[1024,256]{1,0:T(8,128)(2,1)} %param.25) | copy-start | bytes 1572868
  7.7 3.0 %copy-start.23 = (bf16[1024,128]{1,0:T(8,128)(2,1)S(1)}, bf16[1024,128]{1,0:T(8,128)(2,1)}, u32[]{:S(2)}) copy-start(bf16[1024,128]{1,0:T(8,128)(2,1)} %param.26) | copy-start | bytes 786436
  7.7 3.1 %copy-start.24 = (bf16[1024,128]{1,0:T(8,128)(2,1)S(1)}, bf16[1024,128]{1,0:T(8,128)(2,1)}, u32[]{:S(2)}) copy-start(bf16[1024,128]{1,0:T(8,128)(2,1)} %param.27) | copy-start | bytes 786436
  7.8 3.2 %copy-start.27 = (f32[4096]{0:T(1024)S(1)}, f32[4096]{0:T(1024)}, u32[]{:S(2)}) copy-start(f32[4096]{0:T(1024)} %param.18) | copy-start | bytes 49156
  10.4 1.9 copy-start
  12.3 2.7 %copy-start.2 = (bf16[1024,1024]{1,0:T(8,128)(2,1)}, bf16[1024,1024]{1,0:T(8,128)(2,1)S(1)}, u32[]{:S(2)}) copy-start(bf16[1024,1024]{1,0:T(8,128)(2,1)S(1)} %constant_dynamic-update-slice_fusion.w_ref) | copy-start | bytes 6291460
  12.3 2.7 %copy-start.9 = (bf16[256,1024]{1,0:T(8,128)(2,1)S(1)}, bf16[256,1024]{1,0:T(8,128)(2,1)}, u32[]{:S(2)}) copy-start(bf16[256,1024]{1,0:T(8,128)(2,1)} %param.31) | copy-start | bytes 1572868
  12.3 2.7 %copy-start.10 = (bf16[256,1024]{1,0:T(8,128)(2,1)S(1)}, bf16[256,1024]{1,0:T(8,128)(2,1)}, u32[]{:S(2)}) copy-start(bf16[256,1024]{1,0:T(8,128)(2,1)} %param.30) | copy-start | bytes 1572868
  135.7 2.7 %copy-start.32 = (f32[64]{0:T(128)S(1)}, f32[64]{0:T(128)}, u32[]{:S(2)}) copy-start(f32[64]{0:T(128)} %param.23) | copy-start | bytes 772
  138.2 1.9 copy-start.1
  139.1 7.9 %copy-start.31 = (f32[64]{0:T(128)S(1)}, f32[64]{0:T(128)}, u32[]{:S(2)}) copy-start(f32[64]{0:T(128)} %param.22) | copy-start | bytes 772
  140.0 3.4 %copy-start.5 = (bf16[1,384,128]{2,1,0:T(8,128)(2,1)}, bf16[1,384,128]{2,1,0:T(8,128)(2,1)S(1)}, u32[]{:S(2)}) copy-start(bf16[1,384,128]{2,1,0:T(8,128)(2,1)S(1)} %get-tuple-element.69) | copy-start | bytes 294916
  140.1 3.3 %copy-start.3 = (bf16[384,128]{1,0:T(8,128)(2,1)}, bf16[384,128]{1,0:T(8,128)(2,1)S(1)}, u32[]{:S(2)}) copy-start(bf16[384,128]{1,0:T(8,128)(2,1)S(1)} %get-tuple-element.64) | copy-start | bytes 294916
  140.8 43.4 %collective-permute-start = (bf16[2,128,128]{2,1,0:T(8,128)(2,1)}, bf16[2,128,128]{2,1,0:T(8,128)(2,1)}, u32[]{:S(2)}, u32[]{:S(2)}) collective-permute-start(bf16[2,128,128]{2,1,0:T(8,128)(2,1)} %get-tuple-element.87), channel_id=1, source_target_pairs={{0,4},{4,8},{8,12},{1,5},{5,9},{9,13},{2,6},{6,10},{10,14},{3,7},{... | collective-permute-start | bytes 196616 | tf_op jit(solution)/shard_map/ppermute | solution.py:22
  143.5 40.8 %collective-permute-start.1 = (bf16[2,128,128]{2,1,0:T(8,128)(2,1)}, bf16[2,128,128]{2,1,0:T(8,128)(2,1)}, u32[]{:S(2)}, u32[]{:S(2)}) collective-permute-start(bf16[2,128,128]{2,1,0:T(8,128)(2,1)} %get-tuple-element.88), channel_id=1, source_target_pairs={{4,0},{8,4},{12,8},{5,1},{9,5},{13,9},{6,2},{10,6},{14,10},{7,3},{... | collective-permute-start | bytes 196616 | tf_op jit(solution)/shard_map/ppermute | solution.py:25
  147.4 4.2 %copy-start.20 = (bf16[1,384,128]{2,1,0:T(8,128)(2,1)S(1)}, bf16[1,384,128]{2,1,0:T(8,128)(2,1)}, u32[]{:S(2)}) copy-start(bf16[1,384,128]{2,1,0:T(8,128)(2,1)} %get-tuple-element.70) | copy-start | bytes 294916
  151.0 20.7 %copy-start.30 = (f32[256]{0:T(256)S(1)}, f32[256]{0:T(256)}, u32[]{:S(2)}) copy-start(f32[256]{0:T(256)} %mul.387) | copy-start | bytes 3076
  172.7 2.1 copy-start.12
  172.7 2.1 copy-start.14
  172.7 2.1 copy-start.16
  172.7 2.1 copy-start.18
  175.0 6.1 %copy-start.28 = (pred[3,384]{1,0:T(4,128)(4,1)S(1)}, pred[3,384]{1,0:T(4,128)(4,1)}, u32[]{:S(2)}) copy-start(pred[3,384]{1,0:T(4,128)(4,1)} %get-tuple-element.103) | copy-start | bytes 3460
  175.0 6.1 %copy-start.29 = (pred[3,384]{1,0:T(4,128)(4,1)S(1)}, pred[3,384]{1,0:T(4,128)(4,1)}, u32[]{:S(2)}) copy-start(pred[3,384]{1,0:T(4,128)(4,1)} %get-tuple-element.104) | copy-start | bytes 3460
  175.1 6.8 %copy-start.4 = (bf16[384,128]{1,0:T(8,128)(2,1)S(1)}, bf16[384,128]{1,0:T(8,128)(2,1)}, u32[]{:S(2)}) copy-start(bf16[384,128]{1,0:T(8,128)(2,1)} %copy-done.3) | copy-start | bytes 294916
  175.1 7.1 %copy-start.7 = (bf16[384,256]{1,0:T(8,128)(2,1)S(1)}, bf16[384,256]{1,0:T(8,128)(2,1)}, u32[]{:S(2)}) copy-start(bf16[384,256]{1,0:T(8,128)(2,1)} %get-tuple-element.66) | copy-start | bytes 589828
  175.1 7.3 %copy-start.33 = (f32[4]{0:T(128)S(1)}, f32[4]{0:T(128)}, u32[]{:S(2)}) copy-start(f32[4]{0:T(128)} %param.24) | copy-start | bytes 52
  175.1 7.4 %copy-start.19 = (bf16[384,128]{1,0:T(8,128)(2,1)S(1)}, bf16[384,128]{1,0:T(8,128)(2,1)}, u32[]{:S(2)}) copy-start(bf16[384,128]{1,0:T(8,128)(2,1)} %get-tuple-element.68) | copy-start | bytes 294916
  181.1 3.1 %copy-start.6 = (bf16[1,384,128]{2,1,0:T(8,128)(2,1)S(1)}, bf16[1,384,128]{2,1,0:T(8,128)(2,1)}, u32[]{:S(2)}) copy-start(bf16[1,384,128]{2,1,0:T(8,128)(2,1)} %copy-done.5) | copy-start | bytes 294916
  187.7 1.2 copy-start.26
  (5 other events, 3.7 us)
Sparse Core Ops, SparseCore 0:
  202.8 43.6 reduce-scatter.3

commit v2 on v1

v2 whole, which is shorter than its diff:
```python
import functools

import jax
import jax.numpy as jnp
from jax import lax
from jax.experimental import pallas as pl
from jax.experimental.pallas import tpu as pltpu
from jax.sharding import PartitionSpec as P

HD = 64
WINDOW = 128
GRID_W = 64


EPS = 1e-06
THETA = 10000.0


def rope_table(places, width):
    inverse = THETA ** (-jnp.arange(0, width, 2, dtype=jnp.float32) / width)
    angles = places.astype(jnp.float32)[:, None] * inverse[None, :]
    angles = jnp.concatenate([angles, angles], axis=-1)
    return (jnp.cos(angles), jnp.sin(angles))


MESH = pl.DeviceIdType.MESH
HALVES = 2


class LineGather:
    def __init__(self, own, buf, z_recv, r_send, l_send, y_recv=None, y_send=None):
        self.own, self.buf = own, buf
        self.z_recv, self.y_recv = z_recv, y_recv
        self.r_send, self.l_send, self.y_send = r_send, l_send, y_send
        self.n = lax.axis_size("sp")
        self.s = lax.axis_index("sp")
        self.shared = y_recv is not None
        self.g = lax.axis_index("grp") if self.shared else 0
        self.chunks = z_recv.shape[1]
        self.half = buf.shape[1] // HALVES if self.shared else buf.shape[1]
        self.size = self.half // self.chunks

    def rows(self, half, c):
        return pl.ds(pl.multiple_of(half * self.half + c * self.size, self.size), self.size)

    def copy(self, src, o, c, sem, recv, target, half):
        return pltpu.make_async_remote_copy(
            src_ref=src,
            dst_ref=self.buf.at[o, self.rows(half, c)],
            send_sem=sem.at[o, c],
            recv_sem=recv.at[o, c],
            device_id=target,
            device_id_type=MESH,
        )

    def right(self, src, o, c):
        return self.copy(src, o, c, self.r_send, self.z_recv, {"sp": lax.rem(self.s + 1, self.n)}, self.g)

    def left(self, src, o, c):
        return self.copy(
            src, o, c, self.l_send, self.z_recv, {"sp": lax.rem(self.s + self.n - 1, self.n)}, self.g
        )

    def twin(self, o, c, half):
        return self.copy(
            self.buf.at[o, self.rows(half, c)], o, c, self.y_send, self.y_recv, {"grp": 1 - self.g}, half
        )

    def mine(self, c):
        if self.own is None:
            return self.buf.at[self.s, self.rows(self.g, c)]
        return self.own.at[self.rows(self.g, c)]

    def start(self):
        for c in range(self.chunks):
            mine = self.mine(c)

            @pl.when(self.s + 1 < self.n)
            def _():
                self.right(mine, self.s, c).start()

            @pl.when(self.s > 0)
            def _():
                self.left(mine, self.s, c).start()

    def forward(self, d):
        for c in range(self.chunks):

            @pl.when(self.s - d >= 0)
            def _():
                o = self.s - d
                there = self.buf.at[o, self.rows(self.g, c)]
                self.right(there, o, c).wait_recv()

                @pl.when(self.s + 1 < self.n)
                def _():
                    self.right(there, o, c).start()

                if self.shared:
                    self.twin(o, c, self.g).start()

            @pl.when(self.s + d < self.n)
            def _():
                o = self.s + d
                there = self.buf.at[o, self.rows(self.g, c)]
                self.left(there, o, c).wait_recv()

                @pl.when(self.s > 0)
                def _():
                    self.left(there, o, c).start()

                if self.shared:
                    self.twin(o, c, self.g).start()

    def use(self, d, fn):
        @pl.when(self.s - d >= 0)
        def _():
            for c in range(self.chunks):
                self.twin(self.s - d, c, 1 - self.g).wait_recv()
            fn(self.s - d)

        @pl.when(self.s + d < self.n)
        def _():
            for c in range(self.chunks):
                self.twin(self.s + d, c, 1 - self.g).wait_recv()
            fn(self.s + d)

    def run(self, fn):
        self.forward(1)

        @pl.loop(2, self.n)
        def _(d):
            self.forward(d)
            self.use(d - 1, fn)

        self.use(self.n - 1, fn)

    def finish(self):
        @pl.loop(0, self.n)
        def _(o):
            for c in range(self.chunks):
                there = self.buf.at[o, self.rows(self.g, c)]

                @pl.when((o <= self.s) & (self.s + 1 < self.n))
                def _():
                    self.right(there, o, c).wait_send()

                @pl.when((o >= self.s) & (self.s > 0))
                def _():
                    self.left(there, o, c).wait_send()

                if self.shared:

                    @pl.when(o != self.s)
                    def _():
                        self.twin(o, c, self.g).wait_send()


def greet():
    n, s, g = lax.axis_size("sp"), lax.axis_index("sp"), lax.axis_index("grp")
    n_tp, t = lax.axis_size("tp"), lax.axis_index("tp")
    barrier = pltpu.get_barrier_semaphore()
    pl.semaphore_signal(barrier, inc=1, device_id={"grp": 1 - g}, device_id_type=MESH)
    for j in range(1, n_tp):
        pl.semaphore_signal(barrier, inc=1, device_id={"tp": lax.rem(t + j, n_tp)}, device_id_type=MESH)

    @pl.when(s + 1 < n)
    def _():
        pl.semaphore_signal(barrier, inc=1, device_id={"sp": lax.rem(s + 1, n)}, device_id_type=MESH)

    @pl.when(s > 0)
    def _():
        pl.semaphore_signal(barrier, inc=1, device_id={"sp": lax.rem(s + n - 1, n)}, device_id_type=MESH)

    pl.semaphore_wait(barrier, n_tp + (s + 1 < n).astype(jnp.int32) + (s > 0).astype(jnp.int32))


LANES = 128


def by_half(low, high):
    lane = lax.broadcasted_iota(jnp.int32, low.shape, 1)
    return jnp.where(lane < HD, low, high)


def swap_pairs(values, reach):
    lane = lax.broadcasted_iota(jnp.int32, values.shape, 1)
    ahead = pltpu.roll(values, LANES - reach, 1)
    behind = pltpu.roll(values, reach, 1)
    return jnp.where(lax.rem(lane, 2 * reach) < reach, ahead, behind)


def head_tile(tile, kinds, gains_ref, tables_ref):
    square = tile * tile
    zero = jnp.zeros_like(square)
    low = jnp.sum(by_half(square, zero), axis=-1, keepdims=True)
    high = jnp.sum(by_half(zero, square), axis=-1, keepdims=True)
    mean = by_half(jnp.broadcast_to(low, tile.shape), jnp.broadcast_to(high, tile.shape)) * (1.0 / HD)
    scaled = tile * lax.rsqrt(mean + EPS)

    def one(kind):
        if kind is None:
            return tile
        gain, table, reach = kind
        normed = scaled * gains_ref[gain : gain + 1, :]
        return normed * tables_ref[2 * table] + swap_pairs(normed, reach) * tables_ref[2 * table + 1]

    if kinds[0] == kinds[1]:
        return one(kinds[0])
    return by_half(one(kinds[0]), one(kinds[1]))


def layer_kernel(
    sizes, x_ref, gain_ref, w_ref, wo_ref, gains_ref, tables_ref, sink_ref, out_ref,
    xn, proj, wbuf, wo_all, kvd, ext, qs, att, part, rs, halo_recv, halo_send, rs_recv, rs_send, *sems
):
    q_heads, kv_heads = sizes
    n, s = lax.axis_size("sp"), lax.axis_index("sp")
    n_tp, t = lax.axis_size("tp"), lax.axis_index("tp")
    depth = w_ref.shape[0]
    length = x_ref.shape[0]
    into = LineGather(w_ref, wbuf, *sems[:5])
    out = LineGather(wo_ref, wo_all, *sems[5:10])
    keys = LineGather(None, kvd, *sems[10:])
    greet()
    into.start()

    step = 16

    @pl.loop(0, length // step)
    def _(i):
        rows = pl.ds(pl.multiple_of(i * step, step), step)
        values = x_ref[rows, :].astype(jnp.float32)
        mean = jnp.mean(values * values, axis=-1, keepdims=True)
        xn[rows, :] = (values * lax.rsqrt(mean + EPS) * gain_ref[...]).astype(jnp.bfloat16)

    def columns(o):
        return pl.ds(pl.multiple_of(o * depth, depth), depth)

    proj[...] = jnp.dot(xn[:, columns(s)], w_ref[...], preferred_element_type=jnp.float32)

    def add(o):
        proj[...] += jnp.dot(xn[:, columns(o)], wbuf[o], preferred_element_type=jnp.float32)

    into.run(add)

    win_q, win_k, den_q, den_k = (0, 0, 32), (1, 0, 32), (2, 1, 16), (3, 1, 16)
    kinds = (
        [win_q] * q_heads + [den_q] * q_heads + [den_k] * kv_heads + [None] * kv_heads
        + [win_k] * kv_heads + [None] * kv_heads
    )
    q_tiles = 2 * q_heads * HD // LANES
    kv_tiles = 2 * kv_heads * HD // LANES

    def finished(i):
        return head_tile(
            proj[:, i * LANES : (i + 1) * LANES], kinds[2 * i : 2 * i + 2], gains_ref, tables_ref
        )

    for i in range(kv_tiles):
        ext[WINDOW : WINDOW + length, i * LANES : (i + 1) * LANES] = finished(
            q_tiles + kv_tiles + i
        ).astype(jnp.bfloat16)
    for i in range(kv_tiles):
        kvd[s, :, i * LANES : (i + 1) * LANES] = finished(q_tiles + i).astype(jnp.bfloat16)

    def halo(side):
        source = pl.ds(length, WINDOW) if side == 0 else pl.ds(WINDOW, WINDOW)
        target = pl.ds(0, WINDOW) if side == 0 else pl.ds(WINDOW + length, WINDOW)
        peer = lax.rem(s + 1, n) if side == 0 else lax.rem(s + n - 1, n)
        return pltpu.make_async_remote_copy(
            src_ref=ext.at[source], dst_ref=ext.at[target], send_sem=halo_send.at[side],
            recv_sem=halo_recv.at[side], device_id={"sp": peer}, device_id_type=MESH,
        )

    has_right, has_left = s + 1 < n, s > 0

    @pl.when(has_right)
    def _():
        halo(0).start()

    @pl.when(has_left)
    def _():
        halo(1).start()

    keys.start()
    none = jnp.zeros((WINDOW, ext.shape[1]), jnp.bfloat16)

    @pl.when(jnp.logical_not(has_left))
    def _():
        ext[0:WINDOW, :] = none

    @pl.when(jnp.logical_not(has_right))
    def _():
        ext[WINDOW + length : WINDOW + length + WINDOW, :] = none

    group = q_heads // kv_heads

    def place(head):
        return head // 2, head % 2

    for i in range(q_tiles):
        tile = finished(i) * HD ** (-0.5)
        for b in range(2):
            head = 2 * i + b
            half = place((head % q_heads) // group)[1]
            moved = tile if half == b else pltpu.roll(tile, HD, 1)
            zero = jnp.zeros_like(moved)
            kept = by_half(moved, zero) if half == 0 else by_half(zero, moved)
            qs[head] = kept.astype(jnp.bfloat16)

    @pl.when(has_left)
    def _():
        halo(0).wait_recv()

    @pl.when(has_right)
    def _():
        halo(1).wait_recv()

    total_len = length * n

    def joined(results, heads):
        placed = []
        for b in range(2):
            half = place(kv_heads + heads[b] // group)[1]
            placed.append(results[b] if half == b else pltpu.roll(results[b], HD, 1))
        return by_half(placed[0], placed[1]).astype(jnp.bfloat16)

    def tile_of(head):
        return pl.ds(place(head)[0] * LANES, LANES)

    nt = (((1,), (1,)), ((), ()))

    def windowed(pair):
        @pl.loop(0, length // WINDOW)
        def _(b):
            base = pl.multiple_of(b * WINDOW, WINDOW)
            rows = pl.ds(base, WINDOW)
            near = pl.ds(base, 3 * WINDOW)
            shape = (WINDOW, 3 * WINDOW)
            at = lax.broadcasted_iota(jnp.int32, shape, 1) - WINDOW
            away = at - lax.broadcasted_iota(jnp.int32, shape, 0)
            pos = at + (s * length + base)
            valid = (away <= WINDOW) & (away >= -WINDOW) & (pos >= 0) & (pos < total_len)
            results = []
            for head in (2 * pair, 2 * pair + 1):
                key = ext[near, tile_of(head // group)]
                value = ext[near, tile_of(kv_heads + head // group)]
                scores = lax.dot_general(qs[head, rows, :], key, nt, preferred_element_type=jnp.float32)
                scores = jnp.where(valid, scores, -jnp.inf)
                floor = sink_ref[0, head]
                top = jnp.maximum(jnp.max(scores, axis=-1, keepdims=True), floor)
                expon = jnp.exp(scores - top)
                total = jnp.sum(expon, axis=-1, keepdims=True) + jnp.exp(floor - top)
                weights = (expon / total).astype(jnp.bfloat16)
                results.append(jnp.dot(weights, value, preferred_element_type=jnp.float32))
            att[rows, pair * LANES : (pair + 1) * LANES] = joined(results, (2 * pair, 2 * pair + 1))

    pairs = q_heads // 2
    keys.forward(1)
    windowed(0)

    @pl.loop(2, n)
    def _(d):
        keys.forward(d)

    out.start()
    for pair in range(1, pairs):
        windowed(pair)

    def dense(pair):
        @pl.loop(0, length // LANES)
        def _(b):
            rows = pl.ds(pl.multiple_of(b * LANES, LANES), LANES)
            results = []
            for head in (2 * pair, 2 * pair + 1):
                key = kvd[:, :, tile_of(head // group)].reshape(total_len, LANES)
                value = kvd[:, :, tile_of(kv_heads + head // group)].reshape(total_len, LANES)
                scores = lax.dot_general(
                    qs[q_heads + head, rows, :], key, nt, preferred_element_type=jnp.float32
                )
                top = jnp.max(scores, axis=-1, keepdims=True)
                expon = jnp.exp(scores - top)
                total = jnp.sum(expon, axis=-1, keepdims=True)
                summed = jnp.dot(
                    expon.astype(jnp.bfloat16), value, preferred_element_type=jnp.float32
                )
                results.append(summed / total)
            at = (pairs + pair) * LANES
            att[rows, at : at + LANES] = joined(results, (2 * pair, 2 * pair + 1))

    for pair in range(pairs):
        dense(pair)

    share = length // n_tp

    def exchange(o, j):
        peer = lax.rem(t + j, n_tp)
        return pltpu.make_async_remote_copy(
            src_ref=part.at[o, pl.ds(pl.multiple_of(peer * share, share), share)],
            dst_ref=rs.at[t, o], send_sem=rs_send.at[j - 1, o],
            recv_sem=rs_recv.at[t, o], device_id={"tp": peer}, device_id_type=MESH,
        )

    def arrived(o, j):
        source = lax.rem(t + n_tp - j, n_tp)
        return pltpu.make_async_remote_copy(
            src_ref=rs.at[source, o], dst_ref=rs.at[source, o], send_sem=rs_send.at[j - 1, o],
            recv_sem=rs_recv.at[source, o], device_id={"tp": source}, device_id_type=MESH,
        )

    def emit(o, weight):
        part[o] = jnp.dot(att[...], weight, preferred_element_type=jnp.float32).astype(jnp.bfloat16)
        rs[t, o] = part[o, pl.ds(pl.multiple_of(t * share, share), share), :]
        for j in range(1, n_tp):
            exchange(o, j).start()

    def collect(o):
        for j in range(1, n_tp):
            arrived(o, j).wait_recv()
        total = rs[0, o].astype(jnp.float32)
        for g in range(1, n_tp):
            total += rs[g, o].astype(jnp.float32)
        wide = wo_ref.shape[1]
        out_ref[:, pl.ds(pl.multiple_of(o * wide, wide), wide)] = total.astype(jnp.bfloat16)

    emit(s, wo_ref[...])
    out.run(lambda o: emit(o, wo_all[o]))

    @pl.loop(0, n)
    def _(o):
        collect(o)

    @pl.loop(0, n)
    def _(o):
        for j in range(1, n_tp):
            exchange(o, j).wait_send()

    @pl.when(has_right)
    def _():
        halo(0).wait_send()

    @pl.when(has_left)
    def _():
        halo(1).wait_send()

    into.finish()
    out.finish()
    keys.finish()


def local(
    tokens_in,
    norm_gain,
    window_query,
    window_key,
    window_value,
    window_query_gain,
    window_key_gain,
    sink_logit,
    dense_query,
    dense_key,
    dense_value,
    dense_query_gain,
    dense_key_gain,
    window_out,
    dense_out,
):
    length, width = tokens_in.shape
    n, n_tp = lax.axis_size("sp"), lax.axis_size("tp")
    q_heads, kv_heads = window_query.shape[1] // HD, window_key.shape[1] // HD
    weight = jnp.concatenate(
        (window_query, dense_query, dense_key, dense_value, window_key, window_value), axis=1
    )
    weight_out = jnp.concatenate((window_out, dense_out), axis=0)
    gains = jnp.stack(
        [jnp.tile(g, 2) for g in (window_query_gain, window_key_gain, dense_query_gain, dense_key_gain)]
    )
    places = lax.axis_index("sp") * length + jnp.arange(length, dtype=jnp.int32)
    signs = jnp.where(jnp.arange(HD) < HD // 2, -1.0, 1.0)
    cosine, sine = rope_table(places, HD)
    tables = [cosine, sine * signs]
    quarter = jnp.where(jnp.arange(HD // 2) < HD // 4, -1.0, 1.0)
    row_cos, row_sin = rope_table(places // GRID_W, HD // 2)
    col_cos, col_sin = rope_table(places % GRID_W, HD // 2)
    tables.append(jnp.concatenate([row_cos, col_cos], axis=1))
    tables.append(jnp.concatenate([row_sin * quarter, col_sin * quarter], axis=1))
    tables = jnp.stack([jnp.concatenate([table, table], axis=1) for table in tables])
    chunks = 4 if n <= 4 else 1
    gather = [pltpu.SemaphoreType.DMA((n, chunks)) for _ in range(5)]
    kv_cols = 2 * kv_heads * HD
    vmem = pl.BlockSpec(memory_space=pltpu.VMEM)
    share = length // n_tp
    return pl.pallas_call(
        functools.partial(layer_kernel, (q_heads, kv_heads)),
        out_shape=jax.ShapeDtypeStruct((share, width), jnp.bfloat16),
        in_specs=[vmem] * 6 + [pl.BlockSpec(memory_space=pltpu.SMEM)],
        out_specs=vmem,
        scratch_shapes=[
            pltpu.VMEM((length, width), jnp.bfloat16),
            pltpu.VMEM((length, weight.shape[1]), jnp.float32),
            pltpu.VMEM((n,) + weight.shape, jnp.bfloat16),
            pltpu.VMEM((n,) + weight_out.shape, jnp.bfloat16),
            pltpu.VMEM((n, length, kv_cols), jnp.bfloat16),
            pltpu.VMEM((length + 2 * WINDOW, kv_cols), jnp.bfloat16),
            pltpu.VMEM((2 * q_heads, length, LANES), jnp.bfloat16),
            pltpu.VMEM((length, weight_out.shape[0]), jnp.bfloat16),
            pltpu.VMEM((n, length, weight_out.shape[1]), jnp.bfloat16),
            pltpu.VMEM((n_tp, n, share, weight_out.shape[1]), jnp.bfloat16),
            pltpu.SemaphoreType.DMA((2,)),
            pltpu.SemaphoreType.DMA((2,)),
            pltpu.SemaphoreType.DMA((n_tp, n)),
            pltpu.SemaphoreType.DMA((n_tp - 1, n)),
        ]
        + gather
        + gather
        + [pltpu.SemaphoreType.DMA((n, 2 if n <= 4 else 1)) for _ in range(3)],
        compiler_params=pltpu.CompilerParams(
            collective_id=0, has_side_effects=True, vmem_limit_bytes=62 * 1024 * 1024
        ),
    )(tokens_in, norm_gain[None, :], weight, weight_out, gains, tables, sink_logit[None, :])


def solution(mesh):
    return jax.shard_map(
        local,
        mesh=mesh,
        in_specs=(
            P(("grp", "sp"), None),
            P(),
            P("sp", "tp"),
            P("sp", "tp"),
            P("sp", "tp"),
            P(),
            P(),
            P("tp"),
            P("sp", "tp"),
            P("sp", "tp"),
            P("sp", "tp"),
            P(),
            P(),
            P("tp", "sp"),
            P("tp", "sp"),
        ),
        out_specs=P(("grp", "sp", "tp"), None),
        check_vma=False,
    )
```

time: 255 us -> 168 us (0.66)
  waiting for transfers between devices: 43.8 us -> 0 us
  Pallas kernels: 120 us -> 153 us
  blocking collectives: 16.8 us -> 0 us
  other arithmetic: 19 us -> 4.41 us
  between operations: 14.3 us -> 0.17 us
  local copies, waits for them, and re-layouts: 23.8 us -> 10 us
  matrix products: 12 us -> 0 us
  starting transfers between devices: 3.91 us -> 0 us
    reduce_scatter x1 -> x0, waiting for transfers between devices: 43.8 us -> none  [local(): lax.psum_scatter(rounded.astype(jnp.bfloat16), 'tp', scatter_dimension=0,...]
    pallas_call x1, Pallas kernels: 120 us -> 153 us  [local(): pl.pallas_call(functools.partial(layer_kernel, (q_heads, kv_heads)), out_...]
    all_gather x1 -> x0, blocking collectives: 16.8 us -> none  [local(): every = lax.all_gather(dense_pair, 'sp', axis=1, tiled=True)]
    dot_general x9 -> x0, matrix products: 12 us -> none  [the longest x1 5.65 us: local(): jnp.einsum('tk,nkc->tnc', att, out_all, preferred_element_type=jnp.float32)]
    slice x22 -> x0, local copies, waits for them, and re-layouts: 9.39 us -> none  [the longest x7 3.28 us: local(): projected.append(joined[:, at:at + weight.shape[1]])]
    reduce_sum x9 -> x0, other arithmetic: 5.07 us -> none  [the longest x1 2.67 us: local(): jnp.mean(inputs * inputs, axis=-1, keepdims=True) + EPS]
    ppermute x2 -> x0, starting transfers between devices: 3.91 us -> none  [the longest x1 2.63 us: extended(): lax.ppermute(lax.slice_in_dim(block, block.shape[dim] - width, None, axis...]
    convert_element_type x3 -> x0, other arithmetic: 3.73 us -> none  [the longest x1 2.71 us: local(): normed = (inputs * lax.rsqrt(jnp.mean(inputs * inputs, axis=-1, keepdims=...]
  transfers between devices with their start and end apart: 3 -> 0, of which waited for: 1 -> 0; matrix products, arithmetic and copies ran while one was open for 9% -> 0% of each run, Pallas kernels for 0% -> 0%
where the time goes in v2:
time: 168 us; the launch traced here: 167 us
  Pallas kernels  153 us (91%)
  local copies, waits for them, and re-layouts  10 us (6%)
  other arithmetic  4.41 us (3%)
    pallas_call x1, Pallas kernels, local(): pl.pallas_call(functools.partial(layer_kernel, (q_heads, kv_heads)), out_...  153 us
    unnamed x26, local copies, waits for them, and re-layouts  8.42 us

profile of v2, /device:TPU:1, one launch (start us, length us, event | category | flops | bytes accessed | tf_op | source)
XLA Modules:
  0.0 167.3 jit_solution(15843597983236684365)
XLA Ops:
  0.0 0.0 copy-start.5
  0.0 0.0 copy-start
  0.0 2.1 %constant_dynamic-update-slice_fusion.5 = bf16[1024,1024]{1,0:T(8,128)(2,1)} fusion(bf16[1024,256]{1,0:T(8,128)(2,1)} %param.17), kind=kLoop, calls=%fused_computation.23 | loop fusion | bytes 1048576
  2.1 1.9 %constant_dynamic-update-slice_fusion.4 = bf16[1024,1024]{1,0:T(8,128)(2,1)} fusion(bf16[1024,1024]{1,0:T(8,128)(2,1)} %constant_dynamic-update-slice_fusion.5, bf16[1024,256]{1,0:T(8,128)(2,1)} %param.23), kind=kLoop, calls=%fused_computation.22 | loop fusion | bytes 1048576
  4.0 0.0 copy-start.9
  4.1 0.8 constant_dynamic-update-slice_fusion.3
  4.8 0.8 constant_dynamic-update-slice_fusion.2
  5.6 0.7 constant_dynamic-update-slice_fusion.1
  6.4 0.0 copy-done.5
  6.4 0.8 constant_dynamic-update-slice_fusion.w_ref
  7.2 1.0 pad_maximum_fusion.wo_ref
  8.2 0.1 stack_tile.15
  8.3 0.0 copy-done.7
  8.3 0.1 stack_tile.14
  8.4 0.1 stack_tile.13
  8.5 0.1 stack_tile.12
  8.6 0.6 pad_maximum_fusion.5.gains_ref
  9.2 0.1 broadcast_multiply_fusion.4
  9.2 0.1 fusion.2
  9.3 0.1 copy.24
  9.5 0.1 fusion.4
  9.6 0.1 copy.25
  9.8 0.2 maximum_bitcast_fusion.3
  10.0 0.1 copy.21
  10.1 0.1 copy.20
  10.3 0.2 maximum_bitcast_fusion.2
  10.5 0.1 broadcast_multiply_fusion.2
  10.6 0.8 fusion
  11.4 0.2 maximum_bitcast_fusion
  11.6 0.9 pad_maximum_fusion.1.tables_ref
  12.5 152.7 %shard_map.145 = bf16[96,4096]{1,0:T(8,128)(2,1)} custom-call(bf16[384,4096]{1,0:T(8,128)(2,1)} %x_ref.1, f32[1,4096]{1,0:T(1,128)} %bitcast.10, bf16[1024,1024]{1,0:T(8,128)(2,1)} %constant_dynamic-update-slice_fusion.w_ref, bf16[512,1024]{1,0:T(8,128)(2,1)} %pad_maximum_fusion.wo_ref, f32[4,128]{1,0:T(4,128)} %pad_maximum_fusion.5.gains_ref, ...), custom_call_target="tpu_custom_call" | custom-call | tf_op jit(solution)/shard_map/pallas_call | solution.py:494
  165.2 2.1 %copy.32 = bf16[96,4096]{1,0:T(8,128)(2,1)} copy(bf16[96,4096]{1,0:T(8,128)(2,1)} %shard_map.145) | data formatting | bytes 1572864
  (26 shorter events, 0.1 us)
Async XLA Ops:
  0.0 4.0 %copy-start.2 = (bf16[1024,128]{1,0:T(8,128)(2,1)S(1)}, bf16[1024,128]{1,0:T(8,128)(2,1)}, u32[]{:S(2)}) copy-start(bf16[1024,128]{1,0:T(8,128)(2,1)} %param.24) | copy-start | bytes 786436
  0.0 4.8 %copy-start.3 = (bf16[1024,128]{1,0:T(8,128)(2,1)S(1)}, bf16[1024,128]{1,0:T(8,128)(2,1)}, u32[]{:S(2)}) copy-start(bf16[1024,128]{1,0:T(8,128)(2,1)} %param.25) | copy-start | bytes 786436
  0.0 5.6 %copy-start.4 = (bf16[1024,128]{1,0:T(8,128)(2,1)S(1)}, bf16[1024,128]{1,0:T(8,128)(2,1)}, u32[]{:S(2)}) copy-start(bf16[1024,128]{1,0:T(8,128)(2,1)} %param.18) | copy-start | bytes 786436
  0.0 6.4 %copy-start.5 = (bf16[1024,128]{1,0:T(8,128)(2,1)S(1)}, bf16[1024,128]{1,0:T(8,128)(2,1)}, u32[]{:S(2)}) copy-start(bf16[1024,128]{1,0:T(8,128)(2,1)} %param.19) | copy-start | bytes 786436
  0.0 7.1 %copy-start = (bf16[256,1024]{1,0:T(8,128)(2,1)S(1)}, bf16[256,1024]{1,0:T(8,128)(2,1)}, u32[]{:S(2)}) copy-start(bf16[256,1024]{1,0:T(8,128)(2,1)} %param.29) | copy-start | bytes 1572868
  0.0 7.1 %copy-start.1 = (bf16[256,1024]{1,0:T(8,128)(2,1)S(1)}, bf16[256,1024]{1,0:T(8,128)(2,1)}, u32[]{:S(2)}) copy-start(bf16[256,1024]{1,0:T(8,128)(2,1)} %param.28) | copy-start | bytes 1572868
  4.0 4.2 %copy-start.6 = (f32[64]{0:T(128)S(1)}, f32[64]{0:T(128)}, u32[]{:S(2)}) copy-start(f32[64]{0:T(128)} %param.27) | copy-start | bytes 772
  4.0 4.2 %copy-start.7 = (f32[64]{0:T(128)S(1)}, f32[64]{0:T(128)}, u32[]{:S(2)}) copy-start(f32[64]{0:T(128)} %param.26) | copy-start | bytes 772
  4.0 4.3 %copy-start.8 = (f32[64]{0:T(128)S(1)}, f32[64]{0:T(128)}, u32[]{:S(2)}) copy-start(f32[64]{0:T(128)} %param.21) | copy-start | bytes 772
  4.0 4.4 %copy-start.9 = (f32[64]{0:T(128)S(1)}, f32[64]{0:T(128)}, u32[]{:S(2)}) copy-start(f32[64]{0:T(128)} %param.20) | copy-start | bytes 772

commit v3 on v2

--- a/solution.py
+++ b/solution.py
@@ -16,19 +16,12 @@
 THETA = 10000.0
 
 
-def rope_table(places, width):
-    inverse = THETA ** (-jnp.arange(0, width, 2, dtype=jnp.float32) / width)
-    angles = places.astype(jnp.float32)[:, None] * inverse[None, :]
-    angles = jnp.concatenate([angles, angles], axis=-1)
-    return (jnp.cos(angles), jnp.sin(angles))
-
-
 MESH = pl.DeviceIdType.MESH
 HALVES = 2
 
 
 class LineGather:
-    def __init__(self, own, buf, z_recv, r_send, l_send, y_recv=None, y_send=None):
+    def __init__(self, own, buf, z_recv, r_send, l_send, y_recv=None, y_send=None, axis=0):
         self.own, self.buf = own, buf
         self.z_recv, self.y_recv = z_recv, y_recv
         self.r_send, self.l_send, self.y_send = r_send, l_send, y_send
@@ -37,16 +30,22 @@
         self.shared = y_recv is not None
         self.g = lax.axis_index("grp") if self.shared else 0
         self.chunks = z_recv.shape[1]
-        self.half = buf.shape[1] // HALVES if self.shared else buf.shape[1]
+        self.axis = axis
+        extent = buf.shape[1 + axis]
+        self.half = extent // HALVES if self.shared else extent
         self.size = self.half // self.chunks
 
     def rows(self, half, c):
-        return pl.ds(pl.multiple_of(half * self.half + c * self.size, self.size), self.size)
+        piece = pl.ds(pl.multiple_of(half * self.half + c * self.size, self.size), self.size)
+        return (piece,) if self.axis == 0 else (slice(None), piece)
+
+    def block(self, o, half, c):
+        return self.buf.at[(o,) + self.rows(half, c)]
 
     def copy(self, src, o, c, sem, recv, target, half):
         return pltpu.make_async_remote_copy(
             src_ref=src,
-            dst_ref=self.buf.at[o, self.rows(half, c)],
+            dst_ref=self.block(o, half, c),
             send_sem=sem.at[o, c],
             recv_sem=recv.at[o, c],
             device_id=target,
@@ -63,16 +62,16 @@
 
     def twin(self, o, c, half):
         return self.copy(
-            self.buf.at[o, self.rows(half, c)], o, c, self.y_send, self.y_recv, {"grp": 1 - self.g}, half
+            self.block(o, half, c), o, c, self.y_send, self.y_recv, {"grp": 1 - self.g}, half
         )
 
     def mine(self, c):
         if self.own is None:
-            return self.buf.at[self.s, self.rows(self.g, c)]
+            return self.block(self.s, self.g, c)
         return self.own.at[self.rows(self.g, c)]
 
-    def start(self):
-        for c in range(self.chunks):
+    def start(self, first=0, last=None):
+        for c in range(first, self.chunks if last is None else last):
             mine = self.mine(c)
 
             @pl.when(self.s + 1 < self.n)
@@ -89,7 +88,7 @@
             @pl.when(self.s - d >= 0)
             def _():
                 o = self.s - d
-                there = self.buf.at[o, self.rows(self.g, c)]
+                there = self.block(o, self.g, c)
                 self.right(there, o, c).wait_recv()
 
                 @pl.when(self.s + 1 < self.n)
@@ -102,7 +101,7 @@
             @pl.when(self.s + d < self.n)
             def _():
                 o = self.s + d
-                there = self.buf.at[o, self.rows(self.g, c)]
+                there = self.block(o, self.g, c)
                 self.left(there, o, c).wait_recv()
 
                 @pl.when(self.s > 0)
@@ -112,34 +111,39 @@
                 if self.shared:
                     self.twin(o, c, self.g).start()
 
-    def use(self, d, fn):
-        @pl.when(self.s - d >= 0)
-        def _():
-            for c in range(self.chunks):
-                self.twin(self.s - d, c, 1 - self.g).wait_recv()
-            fn(self.s - d)
-
-        @pl.when(self.s + d < self.n)
-        def _():
-            for c in range(self.chunks):
-                self.twin(self.s + d, c, 1 - self.g).wait_recv()
-            fn(self.s + d)
-
-    def run(self, fn):
+    def use(self, d, fn, near=None):
+        for there, o in ((self.s - d >= 0, self.s - d), (self.s + d < self.n, self.s + d)):
+            if near is not None:
+
+                @pl.when(there)
+                def _():
+                    near(o)
+
+        for there, o in ((self.s - d >= 0, self.s - d), (self.s + d < self.n, self.s + d)):
+
+            @pl.when(there)
+            def _():
+                for c in range(self.chunks):
+                    self.twin(o, c, 1 - self.g).wait_recv()
+                fn(o)
+
+    def run(self, fn, near=None, last=None):
         self.forward(1)
 
         @pl.loop(2, self.n)
         def _(d):
             self.forward(d)
-            self.use(d - 1, fn)
-
-        self.use(self.n - 1, fn)
+            self.use(d - 1, fn, near)
+
+        if last is not None:
+            last()
+        self.use(self.n - 1, fn, near)
 
     def finish(self):
         @pl.loop(0, self.n)
         def _(o):
             for c in range(self.chunks):
-                there = self.buf.at[o, self.rows(self.g, c)]
+                there = self.block(o, self.g, c)
 
                 @pl.when((o <= self.s) & (self.s + 1 < self.n))
                 def _():
@@ -211,8 +215,16 @@
 
 
 def layer_kernel(
-    sizes, x_ref, gain_ref, w_ref, wo_ref, gains_ref, tables_ref, sink_ref, out_ref,
-    xn, proj, wbuf, wo_all, kvd, ext, qs, att, part, rs, halo_recv, halo_send, rs_recv, rs_send, *sems
+    sizes, x_ref, gain_ref, small_ref, sink_ref, *refs
+):
+    n_in = sizes[2]
+    in_refs, out_refs = refs[:n_in], refs[n_in : n_in + 2]
+    run_layer(sizes[:2], x_ref, gain_ref, small_ref, sink_ref, in_refs, out_refs, *refs[n_in + 2 :])
+
+
+def run_layer(
+    sizes, x_ref, gain_ref, small_ref, sink_ref, in_refs, out_refs, out_ref,
+    w_ref, wo_ref, tables_ref, load_sem, xn, proj, wbuf, wo_all, kvd, ext, qs, att, part, rs, halo_recv, halo_send, rs_recv, rs_send, *sems
 ):
     q_heads, kv_heads = sizes
     n, s = lax.axis_size("sp"), lax.axis_index("sp")
@@ -220,9 +232,25 @@
     depth = w_ref.shape[0]
     length = x_ref.shape[0]
     into = LineGather(w_ref, wbuf, *sems[:5])
-    out = LineGather(wo_ref, wo_all, *sems[5:10])
+    out = LineGather(wo_ref, wo_all, *sems[5:10], axis=1)
     keys = LineGather(None, kvd, *sems[10:])
+    loads, at = [], 0
+    for ref in in_refs:
+        wide = ref.shape[1]
+        loads.append(
+            pltpu.make_async_copy(ref, w_ref.at[:, at : at + wide], load_sem.at[len(loads)])
+        )
+        at += wide
+    at = 0
+    for ref in out_refs:
+        tall = ref.shape[0]
+        loads.append(pltpu.make_async_copy(ref, wo_ref.at[at : at + tall], load_sem.at[len(loads)]))
+        at += tall
+    for load in loads:
+        load.start()
     greet()
+    for load in loads:
+        load.wait()
     into.start()
 
     step = 16
@@ -239,10 +267,24 @@
 
     proj[...] = jnp.dot(xn[:, columns(s)], w_ref[...], preferred_element_type=jnp.float32)
 
+    band = 64 if length % 64 == 0 else length
+
+    @pl.loop(0, length // band)
+    def _(i):
+        rows = pl.ds(pl.multiple_of(i * band, band), band)
+        shape = (band, LANES)
+        place = lax.broadcasted_iota(jnp.int32, shape, 0) + (s * length + i * band)
+        lane = lax.broadcasted_iota(jnp.int32, shape, 1)
+        spot = jnp.where(lax.rem(lane, HD) < HD // 2, place // GRID_W, lax.rem(place, GRID_W))
+        for k, where in enumerate((place, spot)):
+            angles = where.astype(jnp.float32) * small_ref[4 + k : 5 + k, :]
+            tables_ref[2 * k, rows, :] = jnp.cos(angles)
+            tables_ref[2 * k + 1, rows, :] = jnp.sin(angles) * small_ref[6 + k : 7 + k, :]
+
     def add(o):
         proj[...] += jnp.dot(xn[:, columns(o)], wbuf[o], preferred_element_type=jnp.float32)
 
-    into.run(add)
+    into.run(add, last=lambda: out.start(0, 1))
 
     win_q, win_k, den_q, den_k = (0, 0, 32), (1, 0, 32), (2, 1, 16), (3, 1, 16)
     kinds = (
@@ -254,7 +296,7 @@
 
     def finished(i):
         return head_tile(
-            proj[:, i * LANES : (i + 1) * LANES], kinds[2 * i : 2 * i + 2], gains_ref, tables_ref
+            proj[:, i * LANES : (i + 1) * LANES], kinds[2 * i : 2 * i + 2], small_ref, tables_ref
         )
 
     for i in range(kv_tiles):
@@ -364,7 +406,7 @@
     def _(d):
         keys.forward(d)
 
-    out.start()
+    out.start(1)
     for pair in range(1, pairs):
         windowed(pair)
 
@@ -394,47 +436,64 @@
 
     share = length // n_tp
 
-    def exchange(o, j):
+    wide = wo_ref.shape[1]
+    part_cols = wide // HALVES
+    mine = lax.axis_index("grp")
+
+    def span(h):
+        return pl.ds(pl.multiple_of(h * part_cols, part_cols), part_cols)
+
+    def exchange(o, h, j):
         peer = lax.rem(t + j, n_tp)
         return pltpu.make_async_remote_copy(
-            src_ref=part.at[o, pl.ds(pl.multiple_of(peer * share, share), share)],
-            dst_ref=rs.at[t, o], send_sem=rs_send.at[j - 1, o],
-            recv_sem=rs_recv.at[t, o], device_id={"tp": peer}, device_id_type=MESH,
-        )
-
-    def arrived(o, j):
+            src_ref=part.at[o, pl.ds(pl.multiple_of(peer * share, share), share), span(h)],
+            dst_ref=rs.at[t, o, :, span(h)], send_sem=rs_send.at[j - 1, o, h],
+            recv_sem=rs_recv.at[t, o, h], device_id={"tp": peer}, device_id_type=MESH,
+        )
+
+    def arrived(o, h, j):
         source = lax.rem(t + n_tp - j, n_tp)
+        there = rs.at[source, o, :, span(h)]
         return pltpu.make_async_remote_copy(
-            src_ref=rs.at[source, o], dst_ref=rs.at[source, o], send_sem=rs_send.at[j - 1, o],
-            recv_sem=rs_recv.at[source, o], device_id={"tp": source}, device_id_type=MESH,
-        )
-
-    def emit(o, weight):
-        part[o] = jnp.dot(att[...], weight, preferred_element_type=jnp.float32).astype(jnp.bfloat16)
-        rs[t, o] = part[o, pl.ds(pl.multiple_of(t * share, share), share), :]
+            src_ref=there, dst_ref=there, send_sem=rs_send.at[j - 1, o, h],
+            recv_sem=rs_recv.at[source, o, h], device_id={"tp": source}, device_id_type=MESH,
+        )
+
+    def emit(o, h, weight):
+        part[o, :, span(h)] = jnp.dot(
+            att[...], weight, preferred_element_type=jnp.float32
+        ).astype(jnp.bfloat16)
         for j in range(1, n_tp):
-            exchange(o, j).start()
-
-    def collect(o):
+            exchange(o, h, j).start()
+        rs[t, o, :, span(h)] = part[o, pl.ds(pl.multiple_of(t * share, share), share), span(h)]
+
+    def collect(o, h):
         for j in range(1, n_tp):
-            arrived(o, j).wait_recv()
-        total = rs[0, o].astype(jnp.float32)
+            arrived(o, h, j).wait_recv()
+        total = rs[0, o, :, span(h)].astype(jnp.float32)
         for g in range(1, n_tp):
-            total += rs[g, o].astype(jnp.float32)
-        wide = wo_ref.shape[1]
-        out_ref[:, pl.ds(pl.multiple_of(o * wide, wide), wide)] = total.astype(jnp.bfloat16)
-
-    emit(s, wo_ref[...])
-    out.run(lambda o: emit(o, wo_all[o]))
+            total += rs[g, o, :, span(h)].astype(jnp.float32)
+        columns_out = pl.ds(pl.multiple_of(o * wide + h * part_cols, part_cols), part_cols)
+        out_ref[:, columns_out] = total.astype(jnp.bfloat16)
+
+    for h in range(HALVES):
+        emit(s, h, wo_ref[:, span(h)])
+    out.run(
+        lambda o: emit(o, 1 - mine, wo_all[o, :, span(1 - mine)]),
+        near=lambda o: emit(o, mine, wo_all[o, :, span(mine)]),
+    )
+
+    @pl.loop(0, n)
+    def _(d):
+        o = lax.rem(s + d, n)
+        for h in range(HALVES):
+            collect(o, h)
 
     @pl.loop(0, n)
     def _(o):
-        collect(o)
-
-    @pl.loop(0, n)
-    def _(o):
-        for j in range(1, n_tp):
-            exchange(o, j).wait_send()
+        for h in range(HALVES):
+            for j in range(1, n_tp):
+                exchange(o, h, j).wait_send()
 
     @pl.when(has_right)
     def _():
@@ -469,56 +528,79 @@
     length, width = tokens_in.shape
     n, n_tp = lax.axis_size("sp"), lax.axis_size("tp")
     q_heads, kv_heads = window_query.shape[1] // HD, window_key.shape[1] // HD
-    weight = jnp.concatenate(
-        (window_query, dense_query, dense_key, dense_value, window_key, window_value), axis=1
+    weights, held = [], []
+    for weight in (window_query, dense_query, dense_key, dense_value, window_key, window_value):
+        held.append(weight)
+        if sum(w.shape[1] for w in held) % LANES == 0:
+            weights.append(held[0] if len(held) == 1 else jnp.concatenate(held, axis=1))
+            held = []
+    depth, in_cols = window_query.shape[0], sum(w.shape[1] for w in weights)
+    out_rows, out_cols = window_out.shape[0] + dense_out.shape[0], window_out.shape[1]
+
+    def lanes(row):
+        return jnp.tile(row, LANES // row.shape[0])[None, :]
+
+    def inverse(wide):
+        return THETA ** (-jnp.arange(0, wide, 2, dtype=jnp.float32) / wide)
+
+    def signs(wide):
+        return jnp.where(jnp.arange(wide) < wide // 2, -1.0, 1.0).astype(jnp.float32)
+
+    small = jnp.concatenate(
+        [
+            lanes(window_query_gain),
+            lanes(window_key_gain),
+            lanes(dense_query_gain),
+            lanes(dense_key_gain),
+            lanes(inverse(HD)),
+            lanes(inverse(HD // 2)),
+            lanes(signs(HD)),
+            lanes(signs(HD // 2)),
+        ],
+        axis=0,
     )
-    weight_out = jnp.concatenate((window_out, dense_out), axis=0)
-    gains = jnp.stack(
-        [jnp.tile(g, 2) for g in (window_query_gain, window_key_gain, dense_query_gain, dense_key_gain)]
-    )
-    places = lax.axis_index("sp") * length + jnp.arange(length, dtype=jnp.int32)
-    signs = jnp.where(jnp.arange(HD) < HD // 2, -1.0, 1.0)
-    cosine, sine = rope_table(places, HD)
-    tables = [cosine, sine * signs]
-    quarter = jnp.where(jnp.arange(HD // 2) < HD // 4, -1.0, 1.0)
-    row_cos, row_sin = rope_table(places // GRID_W, HD // 2)
-    col_cos, col_sin = rope_table(places % GRID_W, HD // 2)
-    tables.append(jnp.concatenate([row_cos, col_cos], axis=1))
-    tables.append(jnp.concatenate([row_sin * quarter, col_sin * quarter], axis=1))
-    tables = jnp.stack([jnp.concatenate([table, table], axis=1) for table in tables])
-    chunks = 4 if n <= 4 else 1
-    gather = [pltpu.SemaphoreType.DMA((n, chunks)) for _ in range(5)]
+    def gather(chunks):
+        return [pltpu.SemaphoreType.DMA((n, chunks)) for _ in range(5)]
+
+    in_chunks = 8 if n <= 4 else 1
+    out_chunks = out_cols // HALVES // LANES if n <= 4 else 1
     kv_cols = 2 * kv_heads * HD
     vmem = pl.BlockSpec(memory_space=pltpu.VMEM)
     share = length // n_tp
     return pl.pallas_call(
-        functools.partial(layer_kernel, (q_heads, kv_heads)),
+        functools.partial(layer_kernel, (q_heads, kv_heads, len(weights))),
         out_shape=jax.ShapeDtypeStruct((share, width), jnp.bfloat16),
-        in_specs=[vmem] * 6 + [pl.BlockSpec(memory_space=pltpu.SMEM)],
+        in_specs=[vmem] * 3
+        + [pl.BlockSpec(memory_space=pltpu.SMEM)]
+        + [pl.BlockSpec(memory_space=pl.ANY)] * (len(weights) + 2),
         out_specs=vmem,
         scratch_shapes=[
+            pltpu.VMEM((depth, in_cols), jnp.bfloat16),
+            pltpu.VMEM((out_rows, out_cols), jnp.bfloat16),
+            pltpu.VMEM((4, length, LANES), jnp.float32),
+            pltpu.SemaphoreType.DMA((len(weights) + 2,)),
             pltpu.VMEM((length, width), jnp.bfloat16),
-            pltpu.VMEM((length, weight.shape[1]), jnp.float32),
-            pltpu.VMEM((n,) + weight.shape, jnp.bfloat16),
-            pltpu.VMEM((n,) + weight_out.shape, jnp.bfloat16),
+            pltpu.VMEM((length, in_cols), jnp.float32),
+            pltpu.VMEM((n, depth, in_cols), jnp.bfloat16),
+            pltpu.VMEM((n, out_rows, out_cols), jnp.bfloat16),
             pltpu.VMEM((n, length, kv_cols), jnp.bfloat16),
             pltpu.VMEM((length + 2 * WINDOW, kv_cols), jnp.bfloat16),
             pltpu.VMEM((2 * q_heads, length, LANES), jnp.bfloat16),
-            pltpu.VMEM((length, weight_out.shape[0]), jnp.bfloat16),
-            pltpu.VMEM((n, length, weight_out.shape[1]), jnp.bfloat16),
-            pltpu.VMEM((n_tp, n, share, weight_out.shape[1]), jnp.bfloat16),
+            pltpu.VMEM((length, out_rows), jnp.bfloat16),
+            pltpu.VMEM((n, length, out_cols), jnp.bfloat16),
+            pltpu.VMEM((n_tp, n, share, out_cols), jnp.bfloat16),
             pltpu.SemaphoreType.DMA((2,)),
             pltpu.SemaphoreType.DMA((2,)),
-            pltpu.SemaphoreType.DMA((n_tp, n)),
-            pltpu.SemaphoreType.DMA((n_tp - 1, n)),
+            pltpu.SemaphoreType.DMA((n_tp, n, HALVES)),
+            pltpu.SemaphoreType.DMA((n_tp - 1, n, HALVES)),
         ]
-        + gather
-        + gather
+        + gather(in_chunks)
+        + gather(out_chunks)
         + [pltpu.SemaphoreType.DMA((n, 2 if n <= 4 else 1)) for _ in range(3)],
         compiler_params=pltpu.CompilerParams(
             collective_id=0, has_side_effects=True, vmem_limit_bytes=62 * 1024 * 1024
         ),
-    )(tokens_in, norm_gain[None, :], weight, weight_out, gains, tables, sink_logit[None, :])
+    )(tokens_in, norm_gain[None, :], small, sink_logit[None, :], *weights, window_out, dense_out)
 
 
 def solution(mesh):

time: 168 us -> 159 us (0.946)
  other arithmetic: 4.41 us -> 0.03 us
  local copies, waits for them, and re-layouts: 10 us -> 5.98 us
    unnamed x26 -> x1, local copies, waits for them, and re-layouts: 8.42 us -> 2.06 us
    another operation x8 -> x16, local copies, waits for them, and re-layouts: 0.34 us -> 3.3 us  [lanes(): return jnp.tile(row, LANES // row.shape[0])[None, :]]
    another operation x5 -> x0, other arithmetic: 2.13 us -> none  [the longest x4 1.55 us: local(): jnp.stack([jnp.concatenate([table, table], axis=1) for table in tables])]
where the time goes in v3:
time: 159 us
  Pallas kernels  153 us (96%)
  local copies, waits for them, and re-layouts  5.98 us (4%)
    pallas_call x1, Pallas kernels, local(): pl.pallas_call(functools.partial(layer_kernel, (q_heads, kv_heads, len(we...  153 us
    another operation x16, local copies, waits for them, and re-layouts, lanes(): return jnp.tile(row, LANES // row.shape[0])[None, :]  3.3 us

profile of v3, /device:TPU:1, one launch (start us, length us, event | category | flops | bytes accessed | tf_op | source)
XLA Modules:
  0.0 159.2 jit_solution(2061965569736290454)
XLA Ops:
  0.0 0.1 broadcast_in_dim_tile.30
  0.1 0.7 tile.16
  0.8 0.1 broadcast_in_dim_tile.24
  0.9 0.7 tile.17
  1.5 0.1 broadcast_in_dim_tile.25
  1.6 0.7 tile.18
  2.3 0.1 broadcast_in_dim_tile.26
  2.4 0.7 tile.19
  3.0 0.1 broadcast_in_dim_tile.27
  3.1 0.1 broadcast_in_dim_tile.31
  3.2 0.1 broadcast_in_dim_tile.28
  3.3 0.1 broadcast_in_dim_tile.29
  3.4 0.6 concatenate.3.small_ref
  4.0 153.1 %shard_map.145 = bf16[96,4096]{1,0:T(8,128)(2,1)} custom-call(bf16[384,4096]{1,0:T(8,128)(2,1)} %x_ref.1, f32[1,4096]{1,0:T(1,128)} %bitcast.2, f32[8,128]{1,0:T(8,128)} %concatenate.3.small_ref, f32[1,4]{1,0:T(1,128)} %bitcast.3, bf16[1024,256]{1,0:T(8,128)(2,1)} %refs_0_.1, bf16[1024,256]{1,0:T(8,128)(2,1)} %refs_1_.1, bf16[1024,128]{1,0:T(8,128)(2,1)} %refs_2_.1, ...), custom_call_target="tpu_custom_call" | custom-call | tf_op jit(solution)/shard_map/pallas_call | solution.py:570
  157.1 2.1 %copy.17 = bf16[96,4096]{1,0:T(8,128)(2,1)} copy(bf16[96,4096]{1,0:T(8,128)(2,1)} %shard_map.145) | data formatting | bytes 1572864
  (8 shorter events, 0.0 us)

commit v4 on v3

--- a/solution.py
+++ b/solution.py
@@ -2,6 +2,7 @@
 
 import jax
 import jax.numpy as jnp
+import numpy as np
 from jax import lax
 from jax.experimental import pallas as pl
 from jax.experimental.pallas import tpu as pltpu
@@ -129,7 +130,9 @@
 
     def run(self, fn, near=None, last=None):
         self.forward(1)
-
+        self.rest(fn, near, last)
+
+    def rest(self, fn, near=None, last=None):
         @pl.loop(2, self.n)
         def _(d):
             self.forward(d)
@@ -215,16 +218,16 @@
 
 
 def layer_kernel(
-    sizes, x_ref, gain_ref, small_ref, sink_ref, *refs
+    sizes, x_ref, gain_ref, fixed_ref, g0, g1, g2, g3, sink_ref, *refs
 ):
     n_in = sizes[2]
     in_refs, out_refs = refs[:n_in], refs[n_in : n_in + 2]
-    run_layer(sizes[:2], x_ref, gain_ref, small_ref, sink_ref, in_refs, out_refs, *refs[n_in + 2 :])
+    run_layer(sizes[:2], x_ref, gain_ref, fixed_ref, (g0, g1, g2, g3), sink_ref, in_refs, out_refs, *refs[n_in + 2 :])
 
 
 def run_layer(
-    sizes, x_ref, gain_ref, small_ref, sink_ref, in_refs, out_refs, out_ref,
-    w_ref, wo_ref, tables_ref, load_sem, xn, proj, wbuf, wo_all, kvd, ext, qs, att, part, rs, halo_recv, halo_send, rs_recv, rs_send, *sems
+    sizes, x_ref, gain_ref, fixed_ref, head_gains, sink_ref, in_refs, out_refs, out_ref,
+    small_ref, w_ref, wo_ref, tables_ref, load_sem, xn, proj, wbuf, wo_all, kvd, ext, qs, att, part, rs, halo_recv, halo_send, rs_recv, rs_send, *sems
 ):
     q_heads, kv_heads = sizes
     n, s = lax.axis_size("sp"), lax.axis_index("sp")
@@ -253,6 +256,9 @@
         load.wait()
     into.start()
 
+    for k, ref in enumerate(head_gains):
+        small_ref[k : k + 1, :] = jnp.concatenate([ref[...], ref[...]], axis=1)
+    small_ref[4:8, :] = fixed_ref[...]
     step = 16
 
     @pl.loop(0, length // step)
@@ -431,7 +437,9 @@
             at = (pairs + pair) * LANES
             att[rows, at : at + LANES] = joined(results, (2 * pair, 2 * pair + 1))
 
-    for pair in range(pairs):
+    dense(0)
+    out.forward(1)
+    for pair in range(1, pairs):
         dense(pair)
 
     share = length // n_tp
@@ -478,7 +486,7 @@
 
     for h in range(HALVES):
         emit(s, h, wo_ref[:, span(h)])
-    out.run(
+    out.rest(
         lambda o: emit(o, 1 - mine, wo_all[o, :, span(1 - mine)]),
         near=lambda o: emit(o, mine, wo_all[o, :, span(mine)]),
     )
@@ -537,28 +545,13 @@
     depth, in_cols = window_query.shape[0], sum(w.shape[1] for w in weights)
     out_rows, out_cols = window_out.shape[0] + dense_out.shape[0], window_out.shape[1]
 
-    def lanes(row):
-        return jnp.tile(row, LANES // row.shape[0])[None, :]
-
-    def inverse(wide):
-        return THETA ** (-jnp.arange(0, wide, 2, dtype=jnp.float32) / wide)
-
-    def signs(wide):
-        return jnp.where(jnp.arange(wide) < wide // 2, -1.0, 1.0).astype(jnp.float32)
-
-    small = jnp.concatenate(
-        [
-            lanes(window_query_gain),
-            lanes(window_key_gain),
-            lanes(dense_query_gain),
-            lanes(dense_key_gain),
-            lanes(inverse(HD)),
-            lanes(inverse(HD // 2)),
-            lanes(signs(HD)),
-            lanes(signs(HD // 2)),
-        ],
-        axis=0,
-    )
+    lane = np.arange(LANES)
+    fixed = np.stack(
+        [THETA ** (-2.0 * (lane % (wide // 2)) / wide) for wide in (HD, HD // 2)]
+        + [np.where(lane % wide < wide // 2, -1.0, 1.0) for wide in (HD, HD // 2)]
+    ).astype(np.float32)
+    gains = [g[None, :] for g in (window_query_gain, window_key_gain, dense_query_gain, dense_key_gain)]
+
     def gather(chunks):
         return [pltpu.SemaphoreType.DMA((n, chunks)) for _ in range(5)]
 
@@ -570,11 +563,12 @@
     return pl.pallas_call(
         functools.partial(layer_kernel, (q_heads, kv_heads, len(weights))),
         out_shape=jax.ShapeDtypeStruct((share, width), jnp.bfloat16),
-        in_specs=[vmem] * 3
+        in_specs=[vmem] * 7
         + [pl.BlockSpec(memory_space=pltpu.SMEM)]
         + [pl.BlockSpec(memory_space=pl.ANY)] * (len(weights) + 2),
         out_specs=vmem,
         scratch_shapes=[
+            pltpu.VMEM((8, LANES), jnp.float32),
             pltpu.VMEM((depth, in_cols), jnp.bfloat16),
             pltpu.VMEM((out_rows, out_cols), jnp.bfloat16),
             pltpu.VMEM((4, length, LANES), jnp.float32),
@@ -600,7 +594,7 @@
         compiler_params=pltpu.CompilerParams(
             collective_id=0, has_side_effects=True, vmem_limit_bytes=62 * 1024 * 1024
         ),
-    )(tokens_in, norm_gain[None, :], small, sink_logit[None, :], *weights, window_out, dense_out)
+    )(tokens_in, norm_gain[None, :], fixed, *gains, sink_logit[None, :], *weights, window_out, dense_out)
 
 
 def solution(mesh):

time: 159 us -> 155 us (0.975)
  local copies, waits for them, and re-layouts: 5.98 us -> 2.06 us
    another operation x16 -> x0, local copies, waits for them, and re-layouts: 3.3 us -> none  [lanes(): return jnp.tile(row, LANES // row.shape[0])[None, :]]
where the time goes in v4:
time: 155 us
  Pallas kernels  153 us (99%)
  local copies, waits for them, and re-layouts  2.06 us (1%)
    pallas_call x1, Pallas kernels, local(): pl.pallas_call(functools.partial(layer_kernel, (q_heads, kv_heads, len(we...  153 us

profile of v4, /device:TPU:1, one launch (start us, length us, event | category | flops | bytes accessed | tf_op | source)
XLA Modules:
  0.0 155.3 jit_solution(14210864217597900097)
XLA Ops:
  0.0 153.2 %shard_map.154 = bf16[96,4096]{1,0:T(8,128)(2,1)} custom-call(bf16[384,4096]{1,0:T(8,128)(2,1)} %x_ref.1, f32[1,4096]{1,0:T(1,128)} %bitcast.6, f32[4,128]{1,0:T(4,128)} %constant.2.clone.fixed_ref, f32[1,64]{1,0:T(1,128)} %bitcast.7, f32[1,64]{1,0:T(1,128)} %bitcast.8, f32[1,64]{1,0:T(1,128)} %bitcast.9, f32[1,64]{1,0:T(1,128)} %bitcast.10, ...), custom_call_target="tpu_custom_call" | custom-call | tf_op jit(solution)/shard_map/pallas_call | solution.py:563
  153.2 2.1 %copy.18 = bf16[96,4096]{1,0:T(8,128)(2,1)} copy(bf16[96,4096]{1,0:T(8,128)(2,1)} %shard_map.154) | data formatting | bytes 1572864
